TPU v7x, 32 devices: a whole 2x2x4 slice. The times are simulated.
32 devices in a mesh: sp: 16 (over z, y, core), tp: 2 (over x).
Axes of the slice: x: 2, y: 2, z: 4, core: 2. Of those that a mesh axis runs over, the one named last changes fastest.
Arguments:
- tokens: bfloat16 [4096, 2048], P('sp', 'tp'), may hold values from -64 to 64
- input_norm_gain: float32 [2048], replicated, may hold values from 0.1 to 1.9
- attention_query_weight: bfloat16 [2048, 512], P(None, 'tp'), may hold values from -0.21875 to 0.21875
- attention_key_weight: bfloat16 [2048, 512], P(None, 'tp'), may hold values from -0.21875 to 0.21875
- attention_value_weight: bfloat16 [2048, 512], P(None, 'tp'), may hold values from -0.125 to 0.125
- attention_score_bias: float32 [8], P('tp'), may hold values from -18 to -7
- recurrence_query_weight: bfloat16 [2048, 1024], P(None, 'tp'), may hold values from -0.125 to 0.125
- forget_weight: bfloat16 [2048, 1024], P(None, 'tp'), may hold values from -0.125 to 0.125
- input_weight: bfloat16 [2048, 512], P(None, 'tp'), may hold values from -0.125 to 0.125
- output_gate_weight: bfloat16 [2048, 512], P(None, 'tp'), may hold values from -0.125 to 0.125
- forget_minimum: float32 [8, 128], P('tp'), may hold values from 0.9 to 1
- decay_spikes: float32 [4096, 8], P('sp', 'tp'), may hold values from -2.2 to 0
- head_norm_gain: float32 [64], replicated, may hold values from 0.1 to 1.9
- attention_output_weight: bfloat16 [512, 2048], P('tp'), may hold values from -0.25 to 0.25
- recurrence_output_weight: bfloat16 [512, 2048], P('tp'), may hold values from -0.25 to 0.25
Outputs:
- mixed: bfloat16 [4096, 2048], P('sp', 'tp')
All inputs are finite; a program needn't handle non-finite values.
Results may differ from a plain program's by a relative error of at most 0.018.
Values may be sent and summed in bfloat16 or wider, within the bound.
A program may use at most 64 MiB of HBM per device.

v0:
```python
import jax
import jax.numpy as jnp
from jax import lax
from jax.sharding import PartitionSpec as P

D = 2048
HEAD = 64
REC_KEY = 128
REC_VAL = 64
KEY_SPAN = 1024
REC_SPAN = 64


epsilon = 1e-06


def entering(part, axis, combine, identity):
    place = lax.axis_index(axis)
    gathered = jax.tree.map(lambda a: lax.all_gather(a, axis), part)
    state = jax.tree.map(lambda a, e: jnp.zeros_like(a) + jnp.asarray(e, a.dtype), part, identity)

    def one(hop, state):
        return combine(
            state, jax.tree.map(lambda a: lax.dynamic_index_in_dim(a, hop, 0, False), gathered)
        )

    return lax.fori_loop(0, place, one, state)


def shards(
    tokens,
    input_norm_gain,
    attention_query_weight,
    attention_key_weight,
    attention_value_weight,
    attention_score_bias,
    recurrence_query_weight,
    forget_weight,
    input_weight,
    output_gate_weight,
    forget_minimum,
    decay_spikes,
    head_norm_gain,
    attention_output_weight,
    recurrence_output_weight,
):
    peak_value = lax.Precision.HIGHEST
    row_count = tokens.shape[0]
    weights = (
        attention_query_weight,
        attention_key_weight,
        attention_value_weight,
        recurrence_query_weight,
        forget_weight,
        input_weight,
        output_gate_weight,
    )
    values = lax.all_gather(tokens, "tp", axis=1, tiled=True).astype(jnp.float32)
    scaled = (values * input_norm_gain[None, :]).astype(jnp.bfloat16)
    partials = tuple(
        (jnp.dot(scaled, weight, preferred_element_type=jnp.float32) for weight in weights)
    )
    partials, squares = (partials, jnp.sum(values * values, axis=1))
    inverse = lax.rsqrt(squares / D + epsilon)[:, None]
    query_stick, key_stick, value_stick, query_rows, forget_rows, input_rows, gate_rows = tuple(
        ((running_total * inverse).astype(jnp.bfloat16) for running_total in partials)
    )
    position = lax.axis_index("sp")
    first_row = position * row_count
    end_row = first_row + row_count
    keys_all, values_all = (
        lax.all_gather(key_stick, "sp", axis=0, tiled=True),
        lax.all_gather(value_stick, "sp", axis=0, tiled=True),
    )
    heads_here = attention_score_bias.shape[0]
    query_heads = query_stick.reshape(row_count, heads_here, HEAD)
    query_pos = first_row + jnp.arange(row_count, dtype=jnp.int32)
    block_rows = min(KEY_SPAN, keys_all.shape[0])
    block_count = (end_row + block_rows - 1) // block_rows

    def key_block(block_number, state_carry):
        totals, carried = state_carry
        upper_row = end_row - block_number * block_rows
        lower_row = jnp.maximum(upper_row - block_rows, 0)
        key_rows = lax.dynamic_slice_in_dim(keys_all, lower_row, block_rows, 0).reshape(
            block_rows, heads_here, HEAD
        )
        value_rows = lax.dynamic_slice_in_dim(values_all, lower_row, block_rows, 0).reshape(
            block_rows, heads_here, HEAD
        )
        key_pos = lower_row + jnp.arange(block_rows, dtype=jnp.int32)
        scores = jnp.einsum(
            "qhd,khd->hqk", query_heads, key_rows, preferred_element_type=jnp.float32
        ) * HEAD ** (-0.5)
        scores = scores + attention_score_bias[:, None, None]
        before = ((key_pos[None, :] < query_pos[:, None]) & (key_pos[None, :] < upper_row))[None]
        log_rest = jnp.where(before, jax.nn.log_sigmoid(-scores), 0.0)
        later_sum = lax.cumsum(log_rest, axis=2, reverse=True) - log_rest + carried[:, :, None]
        weights_here = jnp.where(
            before, jnp.exp(jax.nn.log_sigmoid(scores) + later_sum), 0.0
        ).astype(jnp.bfloat16)
        totals = totals + jnp.einsum(
            "hqk,khd->qhd", weights_here, value_rows, preferred_element_type=jnp.float32
        )
        return (totals, carried + jnp.sum(log_rest, axis=2))

    start_carry = (
        jnp.zeros((row_count, heads_here, HEAD), jnp.float32),
        jnp.zeros((heads_here, row_count), jnp.float32),
    )
    totals, carried = lax.fori_loop(0, block_count, key_block, start_carry)
    stick_heads = totals.reshape(row_count, heads_here * HEAD).astype(jnp.bfloat16)
    state_heads_here = forget_minimum.shape[0]
    raised_values = jax.nn.silu(query_rows.astype(jnp.float32)).reshape(
        row_count, state_heads_here, REC_KEY
    )
    admitted_input = (1.0 - forget_minimum)[None] * jax.nn.sigmoid(
        -forget_rows.astype(jnp.float32).reshape(row_count, state_heads_here, REC_KEY)
    )
    forget_logarithm = jnp.log1p(-admitted_input) + decay_spikes[:, :, None]
    inputs = input_rows.astype(jnp.float32).reshape(row_count, state_heads_here, REC_VAL)
    span_count = row_count // REC_SPAN
    causal = jnp.tril(jnp.ones((REC_SPAN, REC_SPAN), jnp.bool_))[:, :, None, None]

    def to_spans(array):
        return array.reshape(span_count, REC_SPAN, state_heads_here, array.shape[-1])

    def advance(state_carry, pieces):
        recurrent_memory, offset = state_carry
        window_query, window_admitted, window_input, span_log = pieces
        running_total = jnp.cumsum(span_log, axis=0)
        log_gaps = running_total[:, None] - running_total[None, :]
        decay_table = jnp.where(causal, jnp.exp(jnp.where(causal, log_gaps, 0.0)), 0.0)
        inner_scores = jnp.einsum(
            "thk,shk,tshk->hts", window_query, window_admitted, decay_table, precision=peak_value
        )
        final_output = jnp.einsum("hts,shv->thv", inner_scores, window_input, precision=peak_value)
        final_output = final_output + jnp.einsum(
            "zbg,bgp->zbp",
            window_query * jnp.exp(running_total),
            recurrent_memory,
            precision=peak_value,
        )
        window_total = running_total[-1]
        recurrent_memory = recurrent_memory * jnp.exp(window_total)[:, :, None] + jnp.einsum(
            "rof,roi->ofi",
            window_admitted * jnp.exp(window_total[None] - running_total),
            window_input,
            precision=peak_value,
        )
        return (
            (recurrent_memory, offset + window_total),
            (final_output, running_total + offset[None]),
        )

    start_state = (
        jnp.zeros((state_heads_here, REC_KEY, REC_VAL), jnp.float32),
        jnp.zeros((state_heads_here, REC_KEY), jnp.float32),
    )
    (memory_end, offset_end), (local_out, prefix_total) = lax.scan(
        advance,
        start_state,
        (
            to_spans(raised_values),
            to_spans(admitted_input),
            to_spans(inputs),
            to_spans(forget_logarithm),
        ),
    )
    local_out = local_out.reshape(row_count, state_heads_here, REC_VAL)
    prefix_total = prefix_total.reshape(row_count, state_heads_here, REC_KEY)
    decay_all = jnp.exp(offset_end)

    def chain_combine(earlier, later_part):
        return (earlier[0] * later_part[0], earlier[1] * later_part[0][:, :, None] + later_part[1])

    identity = (jnp.ones_like(decay_all), jnp.zeros_like(memory_end))
    decay_before, incoming_state = entering((decay_all, memory_end), "sp", chain_combine, identity)
    outputs = local_out + jnp.einsum(
        "zbg,bgp->zbp", raised_values * jnp.exp(prefix_total), incoming_state, precision=peak_value
    )
    normed = (
        outputs
        * lax.rsqrt(jnp.mean(outputs * outputs, axis=2, keepdims=True) + epsilon)
        * head_norm_gain
    )
    gated_out = normed * jax.nn.silu(
        gate_rows.astype(jnp.float32).reshape(row_count, state_heads_here, REC_VAL)
    )
    recurrence_heads = gated_out.reshape(row_count, state_heads_here * REC_VAL).astype(jnp.bfloat16)
    stick_all, state_all = (
        lax.all_gather(stick_heads, "tp", axis=1, tiled=True),
        lax.all_gather(recurrence_heads, "tp", axis=1, tiled=True),
    )
    stick_columns, state_columns = (
        lax.all_to_all(attention_output_weight, "tp", split_axis=1, concat_axis=0, tiled=True),
        lax.all_to_all(recurrence_output_weight, "tp", split_axis=1, concat_axis=0, tiled=True),
    )
    mixed_out = jnp.dot(stick_all, stick_columns, preferred_element_type=jnp.float32)
    mixed_out = (
        mixed_out + jnp.dot(state_all, state_columns, preferred_element_type=jnp.float32)
    ).astype(jnp.bfloat16)
    return mixed_out


def solution(mesh):
    placed = (
        P("sp", "tp"),
        P(),
        P(None, "tp"),
        P(None, "tp"),
        P(None, "tp"),
        P("tp"),
        P(None, "tp"),
        P(None, "tp"),
        P(None, "tp"),
        P(None, "tp"),
        P("tp", None),
        P("sp", "tp"),
        P(),
        P("tp", None),
        P("tp", None),
    )
    return jax.shard_map(
        shards, mesh=mesh, in_specs=placed, out_specs=P("sp", "tp"), check_vma=False
    )
```

profile of v0, /device:TPU:29, one launch (start us, length us, event | category | flops | bytes accessed | tf_op | source)
XLA Modules:
  0.0 390.9 jit_solution(10254816213094781945)
XLA Ops:
  8.9 22.1 %all-gather.8.cloned.1.call-done = bf16[256,2048]{1,0:T(8,128)(2,1)} async-done(((bf16[256,1024]{1,0:T(8,128)(2,1)}), bf16[256,2048]{1,0:T(8,128)(2,1)}) %all-gather.8.cloned.1.call-update) | async-done | bytes 1048592 | tf_op jit(solution)/shard_map/all_gather | solution.py:58
  31.0 1.6 fusion.39
  32.6 2.8 fusion.47
  35.4 2.0 div.42
  37.4 2.4 divide_multiply_fusion
  40.0 1.7 fusion.53
  41.9 1.5 log-plus-one_add_fusion
  43.5 79.1 %while.47 = (s32[]{:T(128)}, f32[4,128,64]{1,2,0:T(8,128)S(1)}, f32[4,128]{1,0:T(4,128)S(1)}, f32[4,64,4,64]{1,0,3,2:T(4,128)}, f32[4,64,4,128]{3,2,1,0:T(4,128)...) while((s32[]{:T(128)}, f32[4,128,64]{1,2,0:T(8,128)S(1)}, ...), condition=%wide.region_8.9_spmd.clone.clone, body=%wide.region_6.8_spmd.clone.clone.sunk | while | flops 77829120 | bytes 20935308 | solution.py:160
  44.2 5.9 %select_bitcast_fusion.2 = f32[4,64,64,128]{3,0,2,1:T(4,128)S(1)} fusion(f32[64,4,128]{2,1,0:T(4,128)S(1)} %fusion.122, pred[64,64]{1,0:T(8,128)(4,1)S(1)} %fusion.124), kind=kLoop, calls=%fused_computation.39.clone.1 | loop fusion | flops 6291456 | bytes 8523776 | tf_op jit(solution)/shard_map/while
  50.1 7.4 %fusion.125 = f32[4,64,64]{1,2,0:T(8,128)S(1)} fusion(f32[4,64,64,128]{3,0,2,1:T(4,128)S(1)} %select_bitcast_fusion.2, f32[4,128,64]{1,2,0:T(8,128)S(1)} %copy.196, f32[4,128,64]{1,2,0:T(8,128)S(1)} %copy.197), kind=kLoop, calls=%fused_computation.38.clone.1 | loop fusion | flops 6275072 | bytes 8716288 | tf_op jit(solution)/shard_map/while/body/eval_jaxpr/thk,shk,tshk->hts/dot_general | solution.py:134
  57.9 4.5 %dynamic_update_slice.16 = f32[4,64,4,64]{1,0,3,2:T(4,128)} dynamic-update-slice(f32[4,64,4,64]{1,0,3,2:T(4,128)} %get-tuple-element.737, f32[1,64,4,64]{1,0,3,2:T(1,128)S(1)} %bitcast.197, s32[]{:T(128)} %get-tuple-element.734, s32[]{:T(128)} %constant.115.clone.1..sunk.2, s32[]{:T(128)} %constant.115.clone.1..sunk.2, s32[]{:T(128)} %constant.115.clone.1..sunk.2) | dynamic-update-slice | bytes 131076 | tf_op jit(solution)/shard_map/while/body/jit(dynamic_update_index_in_dim)/dynamic_update_slice | solution.py:160
  63.9 5.9 %select_bitcast_fusion.2 = f32[4,64,64,128]{3,0,2,1:T(4,128)S(1)} fusion(f32[64,4,128]{2,1,0:T(4,128)S(1)} %fusion.122, pred[64,64]{1,0:T(8,128)(4,1)S(1)} %fusion.124), kind=kLoop, calls=%fused_computation.39.clone.1 | loop fusion | flops 6291456 | bytes 8523776 | tf_op jit(solution)/shard_map/while
  69.9 7.4 %fusion.125 = f32[4,64,64]{1,2,0:T(8,128)S(1)} fusion(f32[4,64,64,128]{3,0,2,1:T(4,128)S(1)} %select_bitcast_fusion.2, f32[4,128,64]{1,2,0:T(8,128)S(1)} %copy.196, f32[4,128,64]{1,2,0:T(8,128)S(1)} %copy.197), kind=kLoop, calls=%fused_computation.38.clone.1 | loop fusion | flops 6275072 | bytes 8716288 | tf_op jit(solution)/shard_map/while/body/eval_jaxpr/thk,shk,tshk->hts/dot_general | solution.py:134
  77.6 4.5 %dynamic_update_slice.16 = f32[4,64,4,64]{1,0,3,2:T(4,128)} dynamic-update-slice(f32[4,64,4,64]{1,0,3,2:T(4,128)} %get-tuple-element.737, f32[1,64,4,64]{1,0,3,2:T(1,128)S(1)} %bitcast.197, s32[]{:T(128)} %get-tuple-element.734, s32[]{:T(128)} %constant.115.clone.1..sunk.2, s32[]{:T(128)} %constant.115.clone.1..sunk.2, s32[]{:T(128)} %constant.115.clone.1..sunk.2) | dynamic-update-slice | bytes 131076 | tf_op jit(solution)/shard_map/while/body/jit(dynamic_update_index_in_dim)/dynamic_update_slice | solution.py:160
  83.6 5.9 %select_bitcast_fusion.2 = f32[4,64,64,128]{3,0,2,1:T(4,128)S(1)} fusion(f32[64,4,128]{2,1,0:T(4,128)S(1)} %fusion.122, pred[64,64]{1,0:T(8,128)(4,1)S(1)} %fusion.124), kind=kLoop, calls=%fused_computation.39.clone.1 | loop fusion | flops 6291456 | bytes 8523776 | tf_op jit(solution)/shard_map/while
  89.6 7.4 %fusion.125 = f32[4,64,64]{1,2,0:T(8,128)S(1)} fusion(f32[4,64,64,128]{3,0,2,1:T(4,128)S(1)} %select_bitcast_fusion.2, f32[4,128,64]{1,2,0:T(8,128)S(1)} %copy.196, f32[4,128,64]{1,2,0:T(8,128)S(1)} %copy.197), kind=kLoop, calls=%fused_computation.38.clone.1 | loop fusion | flops 6275072 | bytes 8716288 | tf_op jit(solution)/shard_map/while/body/eval_jaxpr/thk,shk,tshk->hts/dot_general | solution.py:134
  97.4 4.5 %dynamic_update_slice.16 = f32[4,64,4,64]{1,0,3,2:T(4,128)} dynamic-update-slice(f32[4,64,4,64]{1,0,3,2:T(4,128)} %get-tuple-element.737, f32[1,64,4,64]{1,0,3,2:T(1,128)S(1)} %bitcast.197, s32[]{:T(128)} %get-tuple-element.734, s32[]{:T(128)} %constant.115.clone.1..sunk.2, s32[]{:T(128)} %constant.115.clone.1..sunk.2, s32[]{:T(128)} %constant.115.clone.1..sunk.2) | dynamic-update-slice | bytes 131076 | tf_op jit(solution)/shard_map/while/body/jit(dynamic_update_index_in_dim)/dynamic_update_slice | solution.py:160
  103.4 5.9 %select_bitcast_fusion.2 = f32[4,64,64,128]{3,0,2,1:T(4,128)S(1)} fusion(f32[64,4,128]{2,1,0:T(4,128)S(1)} %fusion.122, pred[64,64]{1,0:T(8,128)(4,1)S(1)} %fusion.124), kind=kLoop, calls=%fused_computation.39.clone.1 | loop fusion | flops 6291456 | bytes 8523776 | tf_op jit(solution)/shard_map/while
  109.3 7.4 %fusion.125 = f32[4,64,64]{1,2,0:T(8,128)S(1)} fusion(f32[4,64,64,128]{3,0,2,1:T(4,128)S(1)} %select_bitcast_fusion.2, f32[4,128,64]{1,2,0:T(8,128)S(1)} %copy.196, f32[4,128,64]{1,2,0:T(8,128)S(1)} %copy.197), kind=kLoop, calls=%fused_computation.38.clone.1 | loop fusion | flops 6275072 | bytes 8716288 | tf_op jit(solution)/shard_map/while/body/eval_jaxpr/thk,shk,tshk->hts/dot_general | solution.py:134
  117.1 4.5 %dynamic_update_slice.16 = f32[4,64,4,64]{1,0,3,2:T(4,128)} dynamic-update-slice(f32[4,64,4,64]{1,0,3,2:T(4,128)} %get-tuple-element.737, f32[1,64,4,64]{1,0,3,2:T(1,128)S(1)} %bitcast.197, s32[]{:T(128)} %get-tuple-element.734, s32[]{:T(128)} %constant.115.clone.1..sunk.2, s32[]{:T(128)} %constant.115.clone.1..sunk.2, s32[]{:T(128)} %constant.115.clone.1..sunk.2) | dynamic-update-slice | bytes 131076 | tf_op jit(solution)/shard_map/while/body/jit(dynamic_update_index_in_dim)/dynamic_update_slice | solution.py:160
  123.3 2.6 fusion.49
  125.9 2.4 copy.121
  128.3 3.6 all-to-all-start
  133.2 11.5 %all-to-all-done = bf16[256,2,1024]{0,2,1:T(8,128)(2,1)S(1)} async-done(((bf16[256,2,1024]{0,2,1:T(8,128)(2,1)}), bf16[256,2,1024]{0,2,1:T(8,128)(2,1)S(1)}, u32[]{:S(2)}, u32[]{:S(2)}) %all-to-all-start) | async-done | bytes 1048608 | tf_op jit(solution)/shard_map/all_to_all | solution.py:196
  144.7 3.6 all-to-all-start.1
  148.4 2.4 fusion.50
  150.8 1.6 copy.122
  152.4 8.0 %all-to-all-done.1 = bf16[256,2,1024]{0,2,1:T(8,128)(2,1)S(1)} async-done(((bf16[256,2,1024]{0,2,1:T(8,128)(2,1)}), bf16[256,2,1024]{0,2,1:T(8,128)(2,1)S(1)}, u32[]{:S(2)}, u32[]{:S(2)}) %all-to-all-start.1) | async-done | bytes 1048608 | tf_op jit(solution)/shard_map/all_to_all | solution.py:197
  160.3 1.3 copy.133
  162.8 1.4 reshape.172
  164.2 1.7 fusion.55
  166.0 1.7 fusion.51
  167.8 19.0 %all-gather.2 = f32[16,4,128]{2,1,0:T(4,128)S(1)} all-gather(f32[1,4,128]{2,1,0:T(4,128)S(1)} %exponential_bitcast_fusion), channel_id=2, replica_groups=mesh['sp'=16,'tp'=2] {'sp'}, dimensions={0}, use_global_device_ids=true | all-gather | bytes 34816 | tf_op jit(solution)/shard_map/all_gather | solution.py:19
  186.9 19.1 %while.45 = (s32[]{:T(128)}, f32[4,128,64]{2,1,0:T(8,128)S(1)}, s32[]{:T(128)}, f32[16,4,128]{2,1,0:T(4,128)S(1)}, f32[16,4,128,64]{2,3,1,0:T(8,128)}, /*index=5*/s32[]{:T(128)}, s32[]{:T(128)}, s32[]{:T(128)}) while((s32[]{:T(128)}, f32[4,128,64]{2,1,0:T(8,128)S(1)}, s32[]{:T(128)}, f32[16,4,128]{2,1,0:T(4,128)S(1)}, ...), condition=%wide.region_10.11_spmd, body=%wide.region_9.10_spmd.sunk | while | flops 65541 | bytes 923775 | solution.py:27
  206.9 5.6 %all_gather.35 = bf16[256,512]{0,1:T(8,128)(2,1)} all-gather(bf16[256,256]{0,1:T(8,128)(2,1)S(1)} %bitcast.205), channel_id=1, replica_groups=mesh['sp'=16,'tp'=2] {'tp'}, dimensions={1}, use_global_device_ids=true | all-gather | bytes 393216 | tf_op jit(solution)/shard_map/all_gather | solution.py:193
  212.4 35.4 %all-gather.12.cloned.1.call-done = bf16[4096,256]{1,0:T(8,128)(2,1)} async-done(((bf16[256,256]{1,0:T(8,128)(2,1)}), bf16[4096,256]{1,0:T(8,128)(2,1)}) %all-gather.12.cloned.1.call-update) | async-done | bytes 2097168 | tf_op jit(solution)/shard_map/all_gather | solution.py:72
  247.8 126.6 %while.46 = (s32[]{:T(128)}, f32[256,4,64]{0,2,1:T(8,128)S(1)}, f32[4,256]{1,0:T(4,128)S(1)}, s32[]{:T(128)}, s32[]{:T(128)}, /*index=5*/bf16[4096,256]{1,0:T(8,...) while((s32[]{:T(128)}, f32[256,4,64]{0,2,1:T(8,128)S(1)}, ...), condition=%wide.region_5.6_spmd.clone, body=%wide.region_1.5_spmd.clone.sunk | while | flops 438962432 | bytes 86642984 | solution.py:111
  248.2 1.5 constant_dynamic-slice_fusion.8
  249.9 5.3 %fusion.111 = (f32[4,256]{1,0:T(4,128)S(1)}, f32[4,256,1024]{1,2,0:T(8,128)S(1)}, f32[4,1024,256]{2,1,0:T(8,128)}) fusion(f32[4]{0:T(128)S(1)} %get-tuple-element.716, pred[256,1024]{0,1:T(8,128)(4,1)S(1)} %compare_and_fusion.2, bf16[1024,4,64]{0,2,1:T(8,128)(2,1)S(1)} %bitcast.196, bf16[256,4,64]{0,2,1:T(8,128)(2,1)S(1)} %get-tuple-element.715), kind=kOutput, calls=%fused_computation.36.clone.1 | convolution fusion | flops 145751040 | bytes 9310224 | tf_op jit(solution)/shard_map/while/body/qhd,khd->hqk/dot_general | solution.py:92
  255.2 10.1 %fusion.112 = f32[4,256,8,128]{1,2,3,0:T(8,128)S(1)} fusion(f32[4,256,8,128]{1,3,2,0:T(8,128)S(1)} %bitcast.194), kind=kOutput, calls=%fused_computation.23.clone.1 | output fusion | flops 133169152 | bytes 8388608 | tf_op jit(solution)/shard_map/reduce-window.6
  265.3 2.0 copy-done.2
  267.3 2.6 broadcast_add_fusion.2
  272.2 6.6 %fusion.113 = bf16[4,256,1024]{1,2,0:T(8,128)(2,1)S(1)} fusion(f32[4,256,8,128]{1,3,2,0:T(8,128)S(1)} %copy.191, f32[4,1024,256]{2,1,0:T(8,128)S(1)} %copy-done.3, f32[4,256]{1,0:T(4,128)S(1)} %get-tuple-element.695, f32[4]{0:T(128)S(1)} %get-tuple-element.716, pred[256,1024]{0,1:T(8,128)(4,1)S(1)} %compare_and_fusion.2), kind=kLoop, calls=%fused_computation.11.clone.1 | loop fusion | flops 24117248 | bytes 10752016 | tf_op jit(solution)/shard_map/while/body/convert_element_type | solution.py:101
  279.9 1.5 constant_dynamic-slice_fusion.8
  281.6 5.3 %fusion.111 = (f32[4,256]{1,0:T(4,128)S(1)}, f32[4,256,1024]{1,2,0:T(8,128)S(1)}, f32[4,1024,256]{2,1,0:T(8,128)}) fusion(f32[4]{0:T(128)S(1)} %get-tuple-element.716, pred[256,1024]{0,1:T(8,128)(4,1)S(1)} %compare_and_fusion.2, bf16[1024,4,64]{0,2,1:T(8,128)(2,1)S(1)} %bitcast.196, bf16[256,4,64]{0,2,1:T(8,128)(2,1)S(1)} %get-tuple-element.715), kind=kOutput, calls=%fused_computation.36.clone.1 | convolution fusion | flops 145751040 | bytes 9310224 | tf_op jit(solution)/shard_map/while/body/qhd,khd->hqk/dot_general | solution.py:92
  286.8 10.1 %fusion.112 = f32[4,256,8,128]{1,2,3,0:T(8,128)S(1)} fusion(f32[4,256,8,128]{1,3,2,0:T(8,128)S(1)} %bitcast.194), kind=kOutput, calls=%fused_computation.23.clone.1 | output fusion | flops 133169152 | bytes 8388608 | tf_op jit(solution)/shard_map/reduce-window.6
  296.9 2.0 copy-done.2
  299.0 2.6 broadcast_add_fusion.2
  303.8 6.6 %fusion.113 = bf16[4,256,1024]{1,2,0:T(8,128)(2,1)S(1)} fusion(f32[4,256,8,128]{1,3,2,0:T(8,128)S(1)} %copy.191, f32[4,1024,256]{2,1,0:T(8,128)S(1)} %copy-done.3, f32[4,256]{1,0:T(4,128)S(1)} %get-tuple-element.695, f32[4]{0:T(128)S(1)} %get-tuple-element.716, pred[256,1024]{0,1:T(8,128)(4,1)S(1)} %compare_and_fusion.2), kind=kLoop, calls=%fused_computation.11.clone.1 | loop fusion | flops 24117248 | bytes 10752016 | tf_op jit(solution)/shard_map/while/body/convert_element_type | solution.py:101
  311.6 1.5 constant_dynamic-slice_fusion.8
  313.2 5.3 %fusion.111 = (f32[4,256]{1,0:T(4,128)S(1)}, f32[4,256,1024]{1,2,0:T(8,128)S(1)}, f32[4,1024,256]{2,1,0:T(8,128)}) fusion(f32[4]{0:T(128)S(1)} %get-tuple-element.716, pred[256,1024]{0,1:T(8,128)(4,1)S(1)} %compare_and_fusion.2, bf16[1024,4,64]{0,2,1:T(8,128)(2,1)S(1)} %bitcast.196, bf16[256,4,64]{0,2,1:T(8,128)(2,1)S(1)} %get-tuple-element.715), kind=kOutput, calls=%fused_computation.36.clone.1 | convolution fusion | flops 145751040 | bytes 9310224 | tf_op jit(solution)/shard_map/while/body/qhd,khd->hqk/dot_general | solution.py:92
  318.5 10.1 %fusion.112 = f32[4,256,8,128]{1,2,3,0:T(8,128)S(1)} fusion(f32[4,256,8,128]{1,3,2,0:T(8,128)S(1)} %bitcast.194), kind=kOutput, calls=%fused_computation.23.clone.1 | output fusion | flops 133169152 | bytes 8388608 | tf_op jit(solution)/shard_map/reduce-window.6
  328.6 2.0 copy-done.2
  330.6 2.6 broadcast_add_fusion.2
  335.5 6.6 %fusion.113 = bf16[4,256,1024]{1,2,0:T(8,128)(2,1)S(1)} fusion(f32[4,256,8,128]{1,3,2,0:T(8,128)S(1)} %copy.191, f32[4,1024,256]{2,1,0:T(8,128)S(1)} %copy-done.3, f32[4,256]{1,0:T(4,128)S(1)} %get-tuple-element.695, f32[4]{0:T(128)S(1)} %get-tuple-element.716, pred[256,1024]{0,1:T(8,128)(4,1)S(1)} %compare_and_fusion.2), kind=kLoop, calls=%fused_computation.11.clone.1 | loop fusion | flops 24117248 | bytes 10752016 | tf_op jit(solution)/shard_map/while/body/convert_element_type | solution.py:101
  343.2 1.5 constant_dynamic-slice_fusion.8
  344.9 5.3 %fusion.111 = (f32[4,256]{1,0:T(4,128)S(1)}, f32[4,256,1024]{1,2,0:T(8,128)S(1)}, f32[4,1024,256]{2,1,0:T(8,128)}) fusion(f32[4]{0:T(128)S(1)} %get-tuple-element.716, pred[256,1024]{0,1:T(8,128)(4,1)S(1)} %compare_and_fusion.2, bf16[1024,4,64]{0,2,1:T(8,128)(2,1)S(1)} %bitcast.196, bf16[256,4,64]{0,2,1:T(8,128)(2,1)S(1)} %get-tuple-element.715), kind=kOutput, calls=%fused_computation.36.clone.1 | convolution fusion | flops 145751040 | bytes 9310224 | tf_op jit(solution)/shard_map/while/body/qhd,khd->hqk/dot_general | solution.py:92
  350.1 10.1 %fusion.112 = f32[4,256,8,128]{1,2,3,0:T(8,128)S(1)} fusion(f32[4,256,8,128]{1,3,2,0:T(8,128)S(1)} %bitcast.194), kind=kOutput, calls=%fused_computation.23.clone.1 | output fusion | flops 133169152 | bytes 8388608 | tf_op jit(solution)/shard_map/reduce-window.6
  360.2 2.0 copy-done.2
  362.3 2.6 broadcast_add_fusion.2
  367.1 6.6 %fusion.113 = bf16[4,256,1024]{1,2,0:T(8,128)(2,1)S(1)} fusion(f32[4,256,8,128]{1,3,2,0:T(8,128)S(1)} %copy.191, f32[4,1024,256]{2,1,0:T(8,128)S(1)} %copy-done.3, f32[4,256]{1,0:T(4,128)S(1)} %get-tuple-element.695, f32[4]{0:T(128)S(1)} %get-tuple-element.716, pred[256,1024]{0,1:T(8,128)(4,1)S(1)} %compare_and_fusion.2), kind=kLoop, calls=%fused_computation.11.clone.1 | loop fusion | flops 24117248 | bytes 10752016 | tf_op jit(solution)/shard_map/while/body/convert_element_type | solution.py:101
  374.5 5.6 %all_gather.30 = bf16[256,512]{0,1:T(8,128)(2,1)S(1)} all-gather(bf16[256,256]{0,1:T(8,128)(2,1)S(1)} %bitcast.204), channel_id=1, replica_groups=mesh['sp'=16,'tp'=2] {'tp'}, dimensions={1}, use_global_device_ids=true | all-gather | bytes 393216 | tf_op jit(solution)/shard_map/all_gather | solution.py:192
  380.1 1.7 fusion.65
  381.8 2.6 fusion.40
  (229 shorter events, 47.1 us)
Async XLA Ops:
  6.5 26.0 %copy-start = (bf16[2048,512]{1,0:T(8,128)(2,1)S(1)}, bf16[2048,512]{1,0:T(8,128)(2,1)}, u32[]{:S(2)}) copy-start(bf16[2048,512]{1,0:T(8,128)(2,1)} %param.28) | copy-start | bytes 6291460
  6.5 24.4 %all-gather.8.cloned.1.call-start = ((), (), s32[]{:S(2)}) async-start(), calls=%async_computation.2 | async-start | bytes 1572864 | tf_op jit(solution)/shard_map/all_gather | solution.py:58
  7.3 179.6 %all-gather.14.cloned.1.call-start = ((), (), s32[]{:S(2)}) async-start(), calls=%async_computation.5 | async-start | bytes 2228224 | tf_op jit(solution)/shard_map/all_gather | solution.py:19
  8.2 29.3 %copy-start.12 = (f32[2048]{0:T(1024)S(1)}, f32[2048]{0:T(1024)}, u32[]{:S(2)}) copy-start(f32[2048]{0:T(1024)} %param.22) | copy-start | bytes 24580
  31.0 6.5 %copy-start.7 = (bf16[256,2048]{1,0:T(8,128)(2,1)S(1)}, bf16[256,2048]{1,0:T(8,128)(2,1)}, u32[]{:S(2)}) copy-start(bf16[256,2048]{1,0:T(8,128)(2,1)} %all-gather.8.cloned.1.call-done) | copy-start | bytes 3145732
  39.8 3.6 copy-start.5
  122.5 0.7 copy-start.4
  122.5 9.4 %copy-start.9 = (bf16[256,2048]{1,0:T(8,128)(2,1)S(1)}, bf16[256,2048]{1,0:T(8,128)(2,1)}, u32[]{:S(2)}) copy-start(bf16[256,2048]{1,0:T(8,128)(2,1)} %param.35) | copy-start | bytes 3145732
  123.2 89.2 %all-gather.10.cloned.1.call-start = ((), (), s32[]{:S(2)}) async-start(), calls=%async_computation.3 | async-start | bytes 2228224 | tf_op jit(solution)/shard_map/all_gather | solution.py:73
  125.9 22.4 %copy-start.8 = (bf16[256,2048]{1,0:T(8,128)(2,1)S(1)}, bf16[256,2048]{1,0:T(8,128)(2,1)}, u32[]{:S(2)}) copy-start(bf16[256,2048]{1,0:T(8,128)(2,1)} %all-gather.8.cloned.1.call-done) | copy-start | bytes 3145732
  128.3 16.4 %all-to-all-start = ((bf16[256,2,1024]{0,2,1:T(8,128)(2,1)}), bf16[256,2,1024]{0,2,1:T(8,128)(2,1)S(1)}, u32[]{:S(2)}, u32[]{:S(2)}) async-start(bf16[256,2,1024]{0,2,1:T(8,128)(2,1)} %bitcast.6), calls=%async_computation | async-start | bytes 2097152 | tf_op jit(solution)/shard_map/all_to_all | solution.py:196
  144.7 15.6 %all-to-all-start.1 = ((bf16[256,2,1024]{0,2,1:T(8,128)(2,1)}), bf16[256,2,1024]{0,2,1:T(8,128)(2,1)S(1)}, u32[]{:S(2)}, u32[]{:S(2)}) async-start(bf16[256,2,1024]{0,2,1:T(8,128)(2,1)} %bitcast.16), calls=%async_computation.1 | async-start | bytes 2097152 | tf_op jit(solution)/shard_map/all_to_all | solution.py:197
  148.3 99.5 %all-gather.12.cloned.1.call-start = ((), (), s32[]{:S(2)}) async-start(), calls=%async_computation.4 | async-start | bytes 2228224 | tf_op jit(solution)/shard_map/all_gather | solution.py:72
  167.7 38.3 %copy-start.6 = (f32[256,512]{1,0:T(8,128)S(1)}, f32[256,512]{1,0:T(8,128)}, u32[]{:S(2)}) copy-start(f32[256,512]{1,0:T(8,128)} %copy-done.5) | copy-start | bytes 1572868
  186.9 19.9 %copy-start.11 = (f32[64]{0:T(128)S(1)}, f32[64]{0:T(128)}, u32[]{:S(2)}) copy-start(f32[64]{0:T(128)} %param.33) | copy-start | bytes 772
  186.9 60.9 %copy-start.10 = (f32[4]{0:T(128)S(1)}, f32[4]{0:T(128)}, u32[]{:S(2)}) copy-start(f32[4]{0:T(128)} %param.26) | copy-start | bytes 52
  265.3 2.0 copy-start.2
  270.0 2.2 copy-start.3
  296.9 2.0 copy-start.2
  301.6 2.2 copy-start.3
  328.6 2.0 copy-start.2
  333.3 2.2 copy-start.3
  360.2 2.0 copy-start.2
  364.9 2.2 copy-start.3
  374.5 9.9 %copy-start.1 = (bf16[2048,512]{1,0:T(8,128)(2,1)S(1)}, bf16[2048,512]{1,0:T(8,128)(2,1)}, u32[]{:S(2)}) copy-start(bf16[2048,512]{1,0:T(8,128)(2,1)} %param.28) | copy-start | bytes 6291460
Sparse Core Ops, SparseCore 0:
  8.9 22.0 all-gather.7
  123.3 39.7 all-gather.13
  165.3 40.2 all-gather.9
  207.6 40.1 all-gather.11
where the time goes:
time: 394 us; the launch traced here: 391 us
  other arithmetic  142 us (36%)
  waiting for transfers between devices  77.7 us (20%)
  local copies, waits for them, and re-layouts  72 us (18%)
  matrix products  46.8 us (12%)
  blocking collectives  30.1 us (8%)
  between operations  13.4 us (3%)
  starting transfers between devices  7.29 us (2%)
    another operation x8, other arithmetic  40.6 us
    all_gather x1, waiting for transfers between devices, shards(): lax.all_gather(key_stick, 'sp', axis=0, tiled=True)  35.4 us
    dot_general x4, other arithmetic, advance(): jnp.einsum('thk,shk,tshk->hts', window_query, window_admitted, decay_tabl...  29.4 us
    convert_element_type x4, other arithmetic, key_block(): weights_here = jnp.where(before, jnp.exp(jax.nn.log_sigmoid(scores) + lat...  26.4 us
    while x4, other arithmetic  23.6 us
    all_gather x1, waiting for transfers between devices, shards(): lax.all_gather(tokens, 'tp', axis=1, tiled=True).astype(jnp.float32)  22.1 us
    dot_general x4, matrix products, key_block(): jnp.einsum('qhd,khd->hqk', query_heads, key_rows, preferred_element_type=...  21.1 us
    all_gather x1, blocking collectives, entering(): gathered = jax.tree.map(lambda a: lax.all_gather(a, axis), part)  19 us
  transfers between devices with their start and end apart: 6, of which 4 were waited for; matrix products, arithmetic and copies ran while one was open for 10% of the time, Pallas kernels for 0%

commit v1 on v0

v1 whole, which is shorter than its diff:
```python
import functools

import jax
import jax.numpy as jnp
from jax import lax
from jax.experimental import pallas as pl
from jax.experimental.pallas import tpu as pltpu
from jax.sharding import PartitionSpec as P

HEAD = 64
REC_KEY = 128
REC_VAL = 64
epsilon = 1e-06
VMEM = pl.BlockSpec(memory_space=pltpu.VMEM)
SMEM = pl.BlockSpec(memory_space=pltpu.SMEM)
NT = (((1,), (1,)), ((), ()))
TN = (((0,), (0,)), ((), ()))


def mm(a, b, dims=(((1,), (0,)), ((), ()))):
    return lax.dot_general(a, b, dims, preferred_element_type=jnp.float32)


def split(x):
    hi = x.astype(jnp.bfloat16)
    return hi, (x - hi.astype(jnp.float32)).astype(jnp.bfloat16)


def iota(shape, dim):
    return lax.broadcasted_iota(jnp.int32, shape, dim)


def local_kernel(q_ref, f_ref, v_ref, low_ref, spike_ref, spike_t_ref, out_ref, qdec_ref, state_ref):
    rows = q_ref.shape[0]
    heads = v_ref.shape[1] // REC_VAL
    r, c = iota((rows, rows), 0), iota((rows, rows), 1)
    causal = r >= c
    lower = causal.astype(jnp.bfloat16)
    upper = (r <= c).astype(jnp.bfloat16)
    hi, lo = split(spike_ref[...])
    spike_col = mm(lower, hi) + mm(lower, lo)
    hi, lo = split(spike_t_ref[...])
    spike_row = mm(hi, upper) + mm(lo, upper)
    for h in range(heads):
        ks = slice(h * REC_KEY, (h + 1) * REC_KEY)
        vs = slice(h * REC_VAL, (h + 1) * REC_VAL)
        q = q_ref[:, ks].astype(jnp.float32)
        lifted = q * jax.nn.sigmoid(q)
        intake = (1.0 - low_ref[:, ks]) * jax.nn.sigmoid(-f_ref[:, ks].astype(jnp.float32))
        hi, lo = split(jnp.log1p(-intake))
        run = mm(lower, hi) + mm(lower, lo)
        s_col = spike_col[:, h : h + 1]
        s_row = spike_row[h : h + 1, :]
        q_up = lifted * jnp.exp(run)
        k_down = (intake * jnp.exp(-run)).astype(jnp.bfloat16)
        decay = jnp.exp(jnp.where(causal, s_col - s_row, 0.0))
        inner = jnp.where(causal, mm(q_up.astype(jnp.bfloat16), k_down, NT) * decay, 0.0)
        v = v_ref[:, vs]
        out_ref[:, vs] = mm(inner.astype(jnp.bfloat16), v)
        qdec_ref[:, ks] = (q_up * jnp.exp(s_col)).astype(jnp.bfloat16)
        total = run[rows - 1 : rows, :] + s_col[rows - 1 : rows, :]
        k_end = (intake * jnp.exp(total - (run + s_col))).astype(jnp.bfloat16)
        state_ref[0:REC_VAL, ks] = mm(v, k_end, TN)
        state_ref[REC_VAL:, ks] = jnp.broadcast_to(total, (8, REC_KEY))


def mix_kernel(bias_ref, q_ref, kv_ref, local_ref, qdec_ref, gate_ref, gain_ref, states_ref, out_ref, acc, carry, state):
    rows, width = q_ref.shape
    heads = width // HEAD
    place = lax.axis_index("sp")
    r, c = iota((rows, rows), 0), iota((rows, rows), 1)
    before = c < r
    sums = jnp.concatenate(
        [(r > c).astype(jnp.bfloat16), jnp.ones((rows, 128), jnp.bfloat16)], axis=1
    )

    def block(number, first):
        for h in range(heads):
            hs = slice(h * HEAD, (h + 1) * HEAD)
            k = kv_ref[number, :, hs]
            v = kv_ref[number, :, width + h * HEAD : width + (h + 1) * HEAD]
            s = mm(q_ref[:, hs] * jnp.bfloat16(HEAD**-0.5), k, NT) + bias_ref[h]
            t = jnp.exp(-jnp.abs(s))
            soft = jnp.where(t < 3.5e-4, t, jnp.log(1.0 + t))
            log_sig = jnp.minimum(s, 0.0) - soft
            rest = log_sig - s
            if first:
                rest = jnp.where(before, rest, 0.0)
            both = mm(rest.astype(jnp.bfloat16), sums)
            later = both[:, :rows]
            if not first:
                later = later + jnp.concatenate([carry[h]] * (rows // 128), axis=1)
            w = jnp.exp(log_sig + later)
            if first:
                w = jnp.where(before, w, 0.0)
            o = mm(w.astype(jnp.bfloat16), v)
            if first:
                acc[:, hs] = o
                carry[h] = both[:, rows:]
            else:
                acc[:, hs] += o
                carry[h] += both[:, rows:]

    block(place, True)

    @pl.loop(0, place)
    def _(step):
        block(place - 1 - step, False)

    out_ref[:, :width] = acc[...].astype(jnp.bfloat16)

    state[...] = jnp.zeros_like(state)

    def earlier(step, suffix):
        number = place - 1 - step
        state[...] += states_ref[number, :REC_VAL, :] * jnp.exp(suffix)
        return suffix + states_ref[number, REC_VAL : REC_VAL + 1, :]

    lax.fori_loop(0, place, earlier, jnp.zeros((1, state.shape[1]), jnp.float32))
    for h in range(local_ref.shape[1] // REC_VAL):
        ks = slice(h * REC_KEY, (h + 1) * REC_KEY)
        vs = slice(h * REC_VAL, (h + 1) * REC_VAL)
        raw = local_ref[:, vs] + mm(qdec_ref[:, ks], state[:, ks].astype(jnp.bfloat16), NT)
        gate = gate_ref[:, vs].astype(jnp.float32)
        mean = jnp.sum(raw * raw, axis=1, keepdims=True) * (1.0 / REC_VAL)
        done = raw * lax.rsqrt(mean + epsilon) * gain_ref[...] * (gate * jax.nn.sigmoid(gate))
        out_ref[:, width + h * REC_VAL : width + (h + 1) * REC_VAL] = done.astype(jnp.bfloat16)


def shards(
    tp,
    tokens,
    input_norm_gain,
    attention_query_weight,
    attention_key_weight,
    attention_value_weight,
    attention_score_bias,
    recurrence_query_weight,
    forget_weight,
    input_weight,
    output_gate_weight,
    forget_minimum,
    decay_spikes,
    head_norm_gain,
    attention_output_weight,
    recurrence_output_weight,
):
    rows = tokens.shape[0]
    mine = lax.axis_index("tp")
    own_rows = jnp.concatenate([attention_output_weight, recurrence_output_weight], axis=0)
    columns = own_rows.shape[1] // tp

    def to_partner(array, shift):
        return lax.ppermute(array, "tp", [(i, (i + shift) % tp) for i in range(tp)])

    def cut(shift):
        return lax.dynamic_slice_in_dim(own_rows, lax.rem(mine + shift, tp) * columns, columns, 1)

    out_weights = [cut(0)] + [to_partner(cut(shift), shift) for shift in range(1, tp)]

    values = lax.all_gather(tokens, "tp", axis=1, tiled=True).astype(jnp.float32)
    scaled = (values * input_norm_gain[None, :]).astype(jnp.bfloat16)
    squares = jnp.mean(values * values, axis=1)
    inverse = lax.rsqrt(squares + epsilon)[:, None]

    def project(weight):
        return (jnp.dot(scaled, weight, preferred_element_type=jnp.float32) * inverse).astype(jnp.bfloat16)

    key_stick, value_stick = project(attention_key_weight), project(attention_value_weight)
    kv_all = lax.all_gather(jnp.concatenate([key_stick, value_stick], axis=1), "sp")
    query_rows, forget_rows = project(recurrence_query_weight), project(forget_weight)
    input_rows = project(input_weight)
    heads_here = forget_minimum.shape[0]
    wide, narrow = heads_here * REC_KEY, heads_here * REC_VAL
    local_out, query_decayed, state_here = pl.pallas_call(
        local_kernel,
        out_shape=(
            jax.ShapeDtypeStruct((rows, narrow), jnp.float32),
            jax.ShapeDtypeStruct((rows, wide), jnp.bfloat16),
            jax.ShapeDtypeStruct((REC_VAL + 8, wide), jnp.float32),
        ),
        in_specs=[VMEM] * 6,
        out_specs=(VMEM,) * 3,
        cost_estimate=pl.CostEstimate(flops=10**9, bytes_accessed=2 * 10**6, transcendentals=10**6),
        name="recurrence_local",
    )(
        query_rows,
        forget_rows,
        input_rows,
        forget_minimum.reshape(1, wide),
        decay_spikes,
        decay_spikes.T,
    )
    states = lax.all_gather(state_here, "sp")
    query_stick, gate_rows = project(attention_query_weight), project(output_gate_weight)
    width = query_stick.shape[1]
    heads = pl.pallas_call(
        mix_kernel,
        out_shape=jax.ShapeDtypeStruct((rows, width + narrow), jnp.bfloat16),
        in_specs=[SMEM] + [VMEM] * 7,
        out_specs=VMEM,
        scratch_shapes=[
            pltpu.VMEM((rows, width), jnp.float32),
            pltpu.VMEM((width // HEAD, rows, 128), jnp.float32),
            pltpu.VMEM((REC_VAL, wide), jnp.float32),
        ],
        compiler_params=pltpu.CompilerParams(vmem_limit_bytes=60 * 1024 * 1024),
        name="mix_heads",
    )(
        attention_score_bias,
        query_stick,
        kv_all,
        local_out,
        query_decayed,
        gate_rows,
        head_norm_gain.reshape(1, REC_VAL),
        states,
    )
    mixed = jnp.dot(heads, out_weights[0], preferred_element_type=jnp.float32)
    for shift in range(1, tp):
        mixed = mixed + jnp.dot(to_partner(heads, shift), out_weights[shift], preferred_element_type=jnp.float32)
    return mixed.astype(jnp.bfloat16)


def solution(mesh):
    placed = (
        P("sp", "tp"),
        P(),
        P(None, "tp"),
        P(None, "tp"),
        P(None, "tp"),
        P("tp"),
        P(None, "tp"),
        P(None, "tp"),
        P(None, "tp"),
        P(None, "tp"),
        P("tp", None),
        P("sp", "tp"),
        P(),
        P("tp", None),
        P("tp", None),
    )
    return jax.shard_map(
        functools.partial(shards, mesh.shape["tp"]),
        mesh=mesh,
        in_specs=placed,
        out_specs=P("sp", "tp"),
        check_vma=False,
    )
```

time: 394 us -> 178 us (0.45)
  other arithmetic: 142 us -> 2.24 us
  local copies, waits for them, and re-layouts: 72 us -> 4.73 us
  matrix products: 46.8 us -> 13.9 us
  waiting for transfers between devices: 77.7 us -> 110 us
  Pallas kernels: 0 us -> 31.6 us
  blocking collectives: 30.1 us -> 0 us
  starting transfers between devices: 7.29 us -> 1.61 us
    another operation x16 -> x0, other arithmetic: 51.3 us -> none
    all_gather x3 -> x2, waiting for transfers between devices: 35.4 us -> 82.9 us  [the longest x1 51.1 us: shards(): lax.all_gather(jnp.concatenate([key_stick, value_stick], axis=1), 'sp')]
    dot_general x30 -> x9, matrix products: 46.8 us -> 13.9 us  [the longest x7 9.74 us: project(): jnp.dot(scaled, weight, preferred_element_type=jnp.float32) * inverse]
    pallas_call x0 -> x2, Pallas kernels: none -> 31.6 us  [the longest x1 27.6 us: shards(): pl.pallas_call(mix_kernel, out_shape=jax.ShapeDtypeStruct((rows, width +...]
    all_gather x3 -> x0, blocking collectives: 30.1 us -> none  [the longest x1 19 us: entering(): gathered = jax.tree.map(lambda a: lax.all_gather(a, axis), part)]
    dot_general x4 -> x0, other arithmetic: 29.4 us -> none  [advance(): jnp.einsum('thk,shk,tshk->hts', window_query, window_admitted, decay_tabl...]
    convert_element_type x6 -> x0, other arithmetic: 26.5 us -> none  [the longest x4 26.4 us: key_block(): weights_here = jnp.where(before, jnp.exp(jax.nn.log_sigmoid(scores) + lat...]
    dynamic_slice x50 -> x1, local copies, waits for them, and re-layouts: 23.7 us -> 0.1 us  [cut(): lax.dynamic_slice_in_dim(own_rows, lax.rem(mine + shift, tp) * columns, c...]
  transfers between devices with their start and end apart: 6 -> 5, of which waited for: 4 -> 4; matrix products, arithmetic and copies ran while one was open for 10% -> 6% of each run, Pallas kernels for 0% -> 16%
where the time goes in v1:
time: 178 us
  waiting for transfers between devices  110 us (62%)
  Pallas kernels  31.6 us (18%)
  matrix products  13.9 us (8%)
  between operations  13.3 us (7%)
  local copies, waits for them, and re-layouts  4.73 us (3%)
  other arithmetic  2.24 us (1%)
    all_gather x1, waiting for transfers between devices, shards(): lax.all_gather(jnp.concatenate([key_stick, value_stick], axis=1), 'sp')  51.1 us
    all_gather x1, waiting for transfers between devices, shards(): states = lax.all_gather(state_here, 'sp')  31.8 us
    pallas_call x1, Pallas kernels, shards(): pl.pallas_call(mix_kernel, out_shape=jax.ShapeDtypeStruct((rows, width +...  27.6 us
    all_gather x1, waiting for transfers between devices, shards(): lax.all_gather(tokens, 'tp', axis=1, tiled=True).astype(jnp.float32)  22.2 us
    dot_general x7, matrix products, project(): jnp.dot(scaled, weight, preferred_element_type=jnp.float32) * inverse  9.74 us
    ppermute x2, waiting for transfers between devices, to_partner(): return lax.ppermute(array, 'tp', [(i, (i + shift) % tp) for i in range(tp)])  4.59 us
    unnamed x24, local copies, waits for them, and re-layouts  4.53 us
    pallas_call x1, Pallas kernels, shards(): pl.pallas_call(local_kernel, out_shape=(jax.ShapeDtypeStruct((rows, narro...  4.01 us
  transfers between devices with their start and end apart: 5, of which 4 were waited for; matrix products, arithmetic and copies ran while one was open for 6% of the time, Pallas kernels for 16%

profile of v1, /device:TPU:29, one launch (start us, length us, event | category | flops | bytes accessed | tf_op | source)
XLA Modules:
  0.0 177.8 jit_solution(9946250649231209530)
XLA Ops:
  6.5 0.0 copy-start
  6.5 0.0 all-gather.6.cloned.1.call-start
  6.5 0.7 all-gather.6.cloned.1.call-update
  7.3 0.0 all-gather.10.cloned.1.call-start
  7.3 1.5 copy.18.spike_ref
  8.8 22.2 %all-gather.6.cloned.1.call-done = bf16[256,2048]{1,0:T(8,128)(2,1)} async-done(((bf16[256,1024]{1,0:T(8,128)(2,1)}), bf16[256,2048]{1,0:T(8,128)(2,1)}) %all-gather.6.cloned.1.call-update) | async-done | bytes 1048592 | tf_op jit(solution)/shard_map/all_gather | solution.py:161
  31.0 1.5 fusion.1
  32.5 0.0 copy-done
  32.5 0.0 copy-start.2
  32.5 0.0 copy-start.5
  32.5 0.0 copy-start.10
  32.5 2.8 %fusion.3.q_ref = bf16[256,512]{1,0:T(8,128)(2,1)} fusion(bf16[2048,512]{1,0:T(8,128)(2,1)S(1)} %copy-done, bf16[256,2048]{1,0:T(8,128)(2,1)} %all-gather.6.cloned.1.call-done, f32[2048]{0:T(1024)} %param.16, f32[256]{0:T(256)S(1)} %add_rsqrt_fusion), kind=kOutput, calls=%fused_computation.8 | convolution fusion | flops 538705920 | bytes 3417088 | tf_op jit(solution)/shard_map/dot_general | solution.py:167
  35.3 0.0 copy-done.2
  35.3 0.0 copy-done.5
  35.3 0.0 copy-done.10
  35.3 0.0 copy-start.6
  35.3 1.4 fusion.4.f_ref
  36.8 0.0 copy-done.6
  36.8 1.1 fusion.8.v_ref
  37.9 4.0 %recurrence_local.1 = (f32[256,256]{1,0:T(8,128)}, bf16[256,512]{1,0:T(8,128)(2,1)}, f32[72,512]{1,0:T(8,128)}) custom-call(bf16[256,512]{1,0:T(8,128)(2,1)} %fusion.3.q_ref, bf16[256,512]{1,0:T(8,128)(2,1)} %fusion.4.f_ref, bf16[256,256]{1,0:T(8,128)(2,1)} %fusion.8.v_ref, f32[1,512]{1,0:T(1,128)} %bitcast.19, f32[256,4]{1,0:T(8,128)} %copy.18.spike_ref, ...), custom_call_target="tpu_custom_call" | custom-call | flops 1000000000 | bytes 2000000 | tf_op jit(solution)/shard_map/recurrence_local/pallas_call | solution.py:175
  41.9 0.0 all-gather.10.cloned.1.call-update
  41.9 0.0 all-gather.8.cloned.1.call-start
  42.0 0.0 copy-start.7
  42.0 1.8 fusion.7
  43.7 0.0 copy-done.7
  43.7 0.4 fusion.6
  44.2 0.0 copy-start.4
  44.2 0.7 pad_maximum_fusion
  44.9 0.0 all-gather.8.cloned.1.call-update
  45.0 1.3 constant_dynamic-update-slice_fusion.1
  46.3 0.0 copy-done.4
  46.3 0.0 copy-start.3
  46.3 0.0 copy-start.8
  46.3 0.1 constant_dynamic-update-slice_fusion
  46.4 0.0 copy-start.1
  46.4 0.0 copy-start.9
  46.4 0.1 constant_dynamic-slice_fusion
  46.5 0.3 collective-permute-start.1
  46.9 1.0 copy-done.3
  47.9 0.7 copy-done.8
  48.6 1.1 fusion.5.q_ref
  49.7 0.0 copy-done.1
  49.7 0.0 copy-done.9
  49.7 1.1 fusion.9.gate_ref
  50.8 31.8 %all-gather.10.cloned.1.call-done = f32[1152,512]{1,0:T(8,128)} async-done(((f32[72,512]{1,0:T(8,128)}), f32[1152,512]{1,0:T(8,128)}) %all-gather.10.cloned.1.call-update) | async-done | bytes 2359312 | tf_op jit(solution)/shard_map/all_gather | solution.py:194
  82.5 51.1 %all-gather.8.cloned.1.call-done = bf16[4096,512]{1,0:T(8,128)(2,1)} async-done(((bf16[256,512]{1,0:T(8,128)(2,1)}), bf16[4096,512]{1,0:T(8,128)(2,1)}) %all-gather.8.cloned.1.call-update) | async-done | bytes 4194320 | tf_op jit(solution)/shard_map/all_gather | solution.py:170
  133.7 27.6 %mix_heads.1 = bf16[256,512]{1,0:T(8,128)(2,1)} custom-call(f32[4]{0:T(128)} %bias_ref.1, bf16[256,256]{1,0:T(8,128)(2,1)} %fusion.5.q_ref, bf16[16,256,512]{2,1,0:T(8,128)(2,1)} %bitcast.15, f32[256,256]{1,0:T(8,128)} %get-tuple-element.8.local_ref, bf16[256,512]{1,0:T(8,128)(2,1)} %get-tuple-element.9.qdec_ref, bf16[256,256]{1,0:T(8,128)(2,1)} %fusion.9.gate_ref, ...), custom_call_target="tpu_custom_call" | custom-call | tf_op jit(solution)/shard_map/mix_heads/pallas_call | solution.py:197
  161.3 1.2 collective-permute-start
  162.5 1.7 fusion.10
  164.2 0.0 collective-permute-done.1
  164.2 4.6 %collective-permute-done = bf16[256,512]{1,0:T(8,128)(2,1)S(1)} collective-permute-done((bf16[256,512]{1,0:T(8,128)(2,1)}, bf16[256,512]{1,0:T(8,128)(2,1)S(1)}, u32[]{:S(2)}, u32[]{:S(2)}) %collective-permute-start) | collective-permute-done | bytes 262176 | tf_op jit(solution)/shard_map/ppermute | solution.py:154
  168.8 2.5 %fusion.2 = bf16[256,1024]{1,0:T(8,128)(2,1)} fusion(f32[256,1024]{1,0:T(8,128)S(1)} %fusion.10, bf16[256,512]{1,0:T(8,128)(2,1)S(1)} %collective-permute-done, bf16[512,1024]{1,0:T(8,128)(2,1)} %collective-permute-done.1), kind=kOutput, calls=%fused_computation.5 | convolution fusion | flops 268959744 | bytes 2883584 | tf_op jit(solution)/shard_map/dot_general | solution.py:221
  (1 shorter events, 0.0 us)
Async XLA Ops:
  6.5 25.9 %copy-start = (bf16[2048,512]{1,0:T(8,128)(2,1)S(1)}, bf16[2048,512]{1,0:T(8,128)(2,1)}, u32[]{:S(2)}) copy-start(bf16[2048,512]{1,0:T(8,128)(2,1)} %param.21) | copy-start | bytes 6291460
  6.5 24.4 %all-gather.6.cloned.1.call-start = ((), (), s32[]{:S(2)}) async-start(), calls=%async_computation | async-start | bytes 1572864 | tf_op jit(solution)/shard_map/all_gather | solution.py:161
  7.3 75.3 %all-gather.10.cloned.1.call-start = ((), (), s32[]{:S(2)}) async-start(), calls=%async_computation.2 | async-start | bytes 2506752 | tf_op jit(solution)/shard_map/all_gather | solution.py:194
  32.5 2.8 %copy-start.2 = (bf16[256,2048]{1,0:T(8,128)(2,1)S(1)}, bf16[256,2048]{1,0:T(8,128)(2,1)}, u32[]{:S(2)}) copy-start(bf16[256,2048]{1,0:T(8,128)(2,1)} %all-gather.6.cloned.1.call-done) | copy-start | bytes 3145732
  32.5 2.8 %copy-start.5 = (bf16[2048,512]{1,0:T(8,128)(2,1)S(1)}, bf16[2048,512]{1,0:T(8,128)(2,1)}, u32[]{:S(2)}) copy-start(bf16[2048,512]{1,0:T(8,128)(2,1)} %param.22) | copy-start | bytes 6291460
  32.5 2.8 %copy-start.10 = (f32[2048]{0:T(1024)S(1)}, f32[2048]{0:T(1024)}, u32[]{:S(2)}) copy-start(f32[2048]{0:T(1024)} %param.16) | copy-start | bytes 24580
  35.3 1.4 copy-start.6
  41.9 91.8 %all-gather.8.cloned.1.call-start = ((), (), s32[]{:S(2)}) async-start(), calls=%async_computation.1 | async-start | bytes 4456448 | tf_op jit(solution)/shard_map/all_gather | solution.py:170
  42.0 1.8 %copy-start.7 = (bf16[2048,256]{1,0:T(8,128)(2,1)S(1)}, bf16[2048,256]{1,0:T(8,128)(2,1)}, u32[]{:S(2)}) copy-start(bf16[2048,256]{1,0:T(8,128)(2,1)} %param.18) | copy-start | bytes 3145732
  44.2 2.1 %copy-start.4 = (bf16[256,2048]{1,0:T(8,128)(2,1)S(1)}, bf16[256,2048]{1,0:T(8,128)(2,1)}, u32[]{:S(2)}) copy-start(bf16[256,2048]{1,0:T(8,128)(2,1)} %param.29) | copy-start | bytes 3145732
  46.3 1.6 copy-start.3
  46.3 2.3 %copy-start.8 = (bf16[2048,256]{1,0:T(8,128)(2,1)S(1)}, bf16[2048,256]{1,0:T(8,128)(2,1)}, u32[]{:S(2)}) copy-start(bf16[2048,256]{1,0:T(8,128)(2,1)} %param.17) | copy-start | bytes 3145732
  46.4 3.3 %copy-start.1 = (bf16[512,2048]{1,0:T(8,128)(2,1)}, bf16[512,2048]{1,0:T(8,128)(2,1)S(1)}, u32[]{:S(2)}) copy-start(bf16[512,2048]{1,0:T(8,128)(2,1)S(1)} %constant_dynamic-update-slice_fusion) | copy-start | bytes 6291460
  46.4 3.3 %copy-start.9 = (bf16[2048,256]{1,0:T(8,128)(2,1)S(1)}, bf16[2048,256]{1,0:T(8,128)(2,1)}, u32[]{:S(2)}) copy-start(bf16[2048,256]{1,0:T(8,128)(2,1)} %param.24) | copy-start | bytes 3145732
  46.5 117.7 %collective-permute-start.1 = (bf16[512,1024]{1,0:T(8,128)(2,1)S(1)}, bf16[512,1024]{1,0:T(8,128)(2,1)}, u32[]{:S(2)}, u32[]{:S(2)}) collective-permute-start(bf16[512,1024]{1,0:T(8,128)(2,1)S(1)} %constant_dynamic-slice_fusion), channel_id=1, source_target_pairs={{0,1},{1,0},{2,3},{3,2},{4,5},{5,4},{6,7},{7,6},{8,9},{9,8},{10,11... | collective-permute-start | bytes 3145736 | tf_op jit(solution)/shard_map/ppermute | solution.py:154
  161.3 7.5 %collective-permute-start = (bf16[256,512]{1,0:T(8,128)(2,1)}, bf16[256,512]{1,0:T(8,128)(2,1)S(1)}, u32[]{:S(2)}, u32[]{:S(2)}) collective-permute-start(bf16[256,512]{1,0:T(8,128)(2,1)} %mix_heads.1), channel_id=1, source_target_pairs={{0,1},{1,0},{2,3},{3,2},{4,5},{5,4},{6,7},{7,6},{8,9},{9,8},{10,11... | collective-permute-start | bytes 786440 | tf_op jit(solution)/shard_map/ppermute | solution.py:154
Sparse Core Ops, SparseCore 0:
  8.9 22.0 all-gather.5
  42.0 40.4 all-gather.9
  84.7 48.9 all-gather.7

commit v2 on v1

--- a/solution.py
+++ b/solution.py
@@ -10,6 +10,7 @@
 HEAD = 64
 REC_KEY = 128
 REC_VAL = 64
+TAIL = 16
 epsilon = 1e-06
 VMEM = pl.BlockSpec(memory_space=pltpu.VMEM)
 SMEM = pl.BlockSpec(memory_space=pltpu.SMEM)
@@ -30,8 +31,13 @@
     return lax.broadcasted_iota(jnp.int32, shape, dim)
 
 
-def local_kernel(q_ref, f_ref, v_ref, low_ref, spike_ref, spike_t_ref, out_ref, qdec_ref, state_ref):
-    rows = q_ref.shape[0]
+def local_kernel(
+    key_ref, value_ref, q_ref, f_ref, v_ref, low_ref, spike_ref, spike_t_ref, out_ref, qdec_ref, pay_ref
+):
+    rows, width = key_ref.shape
+    pay_ref[0:rows, :width] = key_ref[...]
+    pay_ref[0:rows, width:] = value_ref[...]
+    which = iota((TAIL, REC_KEY), 0)
     heads = v_ref.shape[1] // REC_VAL
     r, c = iota((rows, rows), 0), iota((rows, rows), 1)
     causal = r >= c
@@ -60,11 +66,15 @@
         qdec_ref[:, ks] = (q_up * jnp.exp(s_col)).astype(jnp.bfloat16)
         total = run[rows - 1 : rows, :] + s_col[rows - 1 : rows, :]
         k_end = (intake * jnp.exp(total - (run + s_col))).astype(jnp.bfloat16)
-        state_ref[0:REC_VAL, ks] = mm(v, k_end, TN)
-        state_ref[REC_VAL:, ks] = jnp.broadcast_to(total, (8, REC_KEY))
-
-
-def mix_kernel(bias_ref, q_ref, kv_ref, local_ref, qdec_ref, gate_ref, gain_ref, states_ref, out_ref, acc, carry, state):
+        pay_ref[rows : rows + REC_VAL, ks] = mm(v, k_end, TN).astype(jnp.bfloat16)
+        hi, lo = split(total)
+        lo, rest = split(total - hi.astype(jnp.float32))
+        tail = jnp.where(which == 0, hi.astype(jnp.float32), jnp.where(which == 1, lo.astype(jnp.float32), 0.0))
+        tail = jnp.where(which == 2, rest.astype(jnp.float32), tail)
+        pay_ref[rows + REC_VAL :, ks] = tail.astype(jnp.bfloat16)
+
+
+def mix_kernel(bias_ref, q_ref, kv_ref, local_ref, qdec_ref, gate_ref, gain_ref, out_ref, acc, carry, state):
     rows, width = q_ref.shape
     heads = width // HEAD
     place = lax.axis_index("sp")
@@ -77,8 +87,8 @@
     def block(number, first):
         for h in range(heads):
             hs = slice(h * HEAD, (h + 1) * HEAD)
-            k = kv_ref[number, :, hs]
-            v = kv_ref[number, :, width + h * HEAD : width + (h + 1) * HEAD]
+            k = kv_ref[number, :rows, hs]
+            v = kv_ref[number, :rows, width + h * HEAD : width + (h + 1) * HEAD]
             s = mm(q_ref[:, hs] * jnp.bfloat16(HEAD**-0.5), k, NT) + bias_ref[h]
             t = jnp.exp(-jnp.abs(s))
             soft = jnp.where(t < 3.5e-4, t, jnp.log(1.0 + t))
@@ -113,8 +123,9 @@
 
     def earlier(step, suffix):
         number = place - 1 - step
-        state[...] += states_ref[number, :REC_VAL, :] * jnp.exp(suffix)
-        return suffix + states_ref[number, REC_VAL : REC_VAL + 1, :]
+        state[...] += kv_ref[number, rows : rows + REC_VAL, :].astype(jnp.float32) * jnp.exp(suffix)
+        tail = kv_ref[number, rows + REC_VAL :, :].astype(jnp.float32)
+        return suffix + jnp.sum(tail, axis=0, keepdims=True)
 
     lax.fori_loop(0, place, earlier, jnp.zeros((1, state.shape[1]), jnp.float32))
     for h in range(local_ref.shape[1] // REC_VAL):
@@ -127,7 +138,91 @@
         out_ref[:, width + h * REC_VAL : width + (h + 1) * REC_VAL] = done.astype(jnp.bfloat16)
 
 
+def gather_kernel(planes, in_ref, out_ref, own_sem, send_sem, recv_sem):
+    me = lax.axis_index("sp")
+    c, y, z = lax.rem(me, 2), lax.rem(me // 2, 2), me // 4
+    across, other = z * 4 + (1 - y) * 2 + c, z * 4 + y * 2 + (1 - c)
+    ahead = lax.rem(z + 1, planes) * 4 + y * 2 + c
+    behind = lax.rem(z + planes - 1, planes) * 4 + y * 2 + c
+    barrier = pltpu.get_barrier_semaphore()
+    for neighbour in (across, other, ahead, behind):
+        pl.semaphore_signal(barrier, inc=1, device_id={"sp": neighbour}, device_id_type=pl.DeviceIdType.MESH)
+    own = pltpu.make_async_copy(in_ref, out_ref.at[me], own_sem)
+    own.start()
+    pl.semaphore_wait(barrier, 4)
+    own.wait()
+
+    def copy(number, way, target):
+        return pltpu.make_async_remote_copy(
+            src_ref=out_ref.at[number],
+            dst_ref=out_ref.at[number],
+            send_sem=send_sem.at[way, number],
+            recv_sem=recv_sem.at[number],
+            device_id={"sp": target},
+            device_id_type=pl.DeviceIdType.MESH,
+        )
+
+    def column(d):
+        return (z - d) * 4 + y * 2 + c
+
+    def facing(d):
+        return (z - d) * 4 + (1 - y) * 2 + c
+
+    def column_sends(d, act):
+        @pl.when(z < planes - 1)
+        def _():
+            act(copy(column(d), 0, ahead))
+
+        @pl.when((d > 0) | (y == 0))
+        def _():
+            act(copy(column(d), 1, across))
+
+        @pl.when((d > 0) | (c == 0))
+        def _():
+            act(copy(column(d), 2, other))
+
+    def facing_sends(d, act):
+        @pl.when((d > 0) | (y == 1))
+        def _():
+            act(copy(facing(d), 2, other))
+
+    def start(one):
+        one.start()
+
+    @pl.loop(0, z + 2)
+    def _(d):
+        @pl.when(d <= z)
+        def _():
+            @pl.when(d > 0)
+            def _():
+                copy(column(d), 0, ahead).wait_recv()
+
+            column_sends(d, start)
+
+        @pl.when(d > 0)
+        def _():
+            @pl.when((d > 1) | (y == 1))
+            def _():
+                copy(facing(d - 1), 1, across).wait_recv()
+
+            facing_sends(d - 1, start)
+
+    @pl.loop(0, z + 1)
+    def _(d):
+        @pl.when((d > 0) | (c == 1))
+        def _():
+            copy((z - d) * 4 + y * 2 + 1 - c, 2, other).wait_recv()
+
+        @pl.when((d > 0) | (y == 1))
+        def _():
+            copy((z - d) * 4 + (1 - y) * 2 + 1 - c, 2, other).wait_recv()
+
+        column_sends(d, lambda one: one.wait_send())
+        facing_sends(d, lambda one: one.wait_send())
+
+
 def shards(
+    sp,
     tp,
     tokens,
     input_norm_gain,
@@ -147,18 +242,27 @@
 ):
     rows = tokens.shape[0]
     mine = lax.axis_index("tp")
+
+    def to_partner(array, shift):
+        return lax.ppermute(array, "tp", [(i, (i + shift) % tp) for i in range(tp)])
+
+    features = tokens.shape[1]
+    values = jnp.zeros((rows, features * tp), tokens.dtype)
+    for shift in range(tp):
+        piece = tokens if shift == 0 else to_partner(tokens, shift)
+        values = lax.dynamic_update_slice_in_dim(values, piece, lax.rem(mine + tp - shift, tp) * features, 1)
+    attention_output_weight, recurrence_output_weight, values = lax.optimization_barrier(
+        (attention_output_weight, recurrence_output_weight, values)
+    )
     own_rows = jnp.concatenate([attention_output_weight, recurrence_output_weight], axis=0)
     columns = own_rows.shape[1] // tp
 
-    def to_partner(array, shift):
-        return lax.ppermute(array, "tp", [(i, (i + shift) % tp) for i in range(tp)])
-
     def cut(shift):
         return lax.dynamic_slice_in_dim(own_rows, lax.rem(mine + shift, tp) * columns, columns, 1)
 
     out_weights = [cut(0)] + [to_partner(cut(shift), shift) for shift in range(1, tp)]
 
-    values = lax.all_gather(tokens, "tp", axis=1, tiled=True).astype(jnp.float32)
+    values = values.astype(jnp.float32)
     scaled = (values * input_norm_gain[None, :]).astype(jnp.bfloat16)
     squares = jnp.mean(values * values, axis=1)
     inverse = lax.rsqrt(squares + epsilon)[:, None]
@@ -167,23 +271,24 @@
         return (jnp.dot(scaled, weight, preferred_element_type=jnp.float32) * inverse).astype(jnp.bfloat16)
 
     key_stick, value_stick = project(attention_key_weight), project(attention_value_weight)
-    kv_all = lax.all_gather(jnp.concatenate([key_stick, value_stick], axis=1), "sp")
     query_rows, forget_rows = project(recurrence_query_weight), project(forget_weight)
     input_rows = project(input_weight)
     heads_here = forget_minimum.shape[0]
     wide, narrow = heads_here * REC_KEY, heads_here * REC_VAL
-    local_out, query_decayed, state_here = pl.pallas_call(
+    local_out, query_decayed, payload = pl.pallas_call(
         local_kernel,
         out_shape=(
             jax.ShapeDtypeStruct((rows, narrow), jnp.float32),
             jax.ShapeDtypeStruct((rows, wide), jnp.bfloat16),
-            jax.ShapeDtypeStruct((REC_VAL + 8, wide), jnp.float32),
+            jax.ShapeDtypeStruct((rows + REC_VAL + TAIL, wide), jnp.bfloat16),
         ),
-        in_specs=[VMEM] * 6,
+        in_specs=[VMEM] * 8,
         out_specs=(VMEM,) * 3,
         cost_estimate=pl.CostEstimate(flops=10**9, bytes_accessed=2 * 10**6, transcendentals=10**6),
         name="recurrence_local",
     )(
+        key_stick,
+        value_stick,
         query_rows,
         forget_rows,
         input_rows,
@@ -191,13 +296,26 @@
         decay_spikes,
         decay_spikes.T,
     )
-    states = lax.all_gather(state_here, "sp")
+    kv_all = pl.pallas_call(
+        functools.partial(gather_kernel, sp // 4),
+        out_shape=jax.ShapeDtypeStruct((sp,) + payload.shape, payload.dtype),
+        in_specs=[VMEM],
+        out_specs=VMEM,
+        scratch_shapes=[
+            pltpu.SemaphoreType.DMA,
+            pltpu.SemaphoreType.DMA((3, sp)),
+            pltpu.SemaphoreType.DMA((sp,)),
+        ],
+        compiler_params=pltpu.CompilerParams(collective_id=0, has_side_effects=True),
+        cost_estimate=pl.CostEstimate(flops=10**10, bytes_accessed=10**8, transcendentals=0),
+        name="gather_earlier",
+    )(payload)
     query_stick, gate_rows = project(attention_query_weight), project(output_gate_weight)
     width = query_stick.shape[1]
     heads = pl.pallas_call(
         mix_kernel,
         out_shape=jax.ShapeDtypeStruct((rows, width + narrow), jnp.bfloat16),
-        in_specs=[SMEM] + [VMEM] * 7,
+        in_specs=[SMEM] + [VMEM] * 6,
         out_specs=VMEM,
         scratch_shapes=[
             pltpu.VMEM((rows, width), jnp.float32),
@@ -214,7 +332,6 @@
         query_decayed,
         gate_rows,
         head_norm_gain.reshape(1, REC_VAL),
-        states,
     )
     mixed = jnp.dot(heads, out_weights[0], preferred_element_type=jnp.float32)
     for shift in range(1, tp):
@@ -241,7 +358,7 @@
         P("tp", None),
     )
     return jax.shard_map(
-        functools.partial(shards, mesh.shape["tp"]),
+        functools.partial(shards, mesh.shape["sp"], mesh.shape["tp"]),
         mesh=mesh,
         in_specs=placed,
         out_specs=P("sp", "tp"),

time: 178 us -> 105 us (0.59)
  waiting for transfers between devices: 110 us -> 14.5 us
  Pallas kernels: 31.6 us -> 69.7 us
  between operations: 13.3 us -> 0.11 us
  other arithmetic: 2.24 us -> 0.29 us
    all_gather x3 -> x0, waiting for transfers between devices: 105 us -> none  [the longest x1 51.1 us: shards(): lax.all_gather(jnp.concatenate([key_stick, value_stick], axis=1), 'sp')]
    pallas_call x0 -> x1, Pallas kernels: none -> 38.3 us  [shards(): pl.pallas_call(functools.partial(gather_kernel, sp // 4), out_shape=jax.S...]
    ppermute x2 -> x3, waiting for transfers between devices: 4.59 us -> 14.5 us  [to_partner(): return lax.ppermute(array, 'tp', [(i, (i + shift) % tp) for i in range(tp)])]
  transfers between devices with their start and end apart: 5 -> 3, of which waited for: 4 -> 2; matrix products, arithmetic and copies ran while one was open for 6% -> 4% of each run, Pallas kernels for 16% -> 67%
where the time goes in v2:
time: 105 us
  Pallas kernels  69.7 us (66%)
  waiting for transfers between devices  14.5 us (14%)
  matrix products  12.6 us (12%)
  local copies, waits for them, and re-layouts  4.73 us (5%)
  starting transfers between devices  2.72 us (3%)
    pallas_call x1, Pallas kernels, shards(): pl.pallas_call(functools.partial(gather_kernel, sp // 4), out_shape=jax.S...  38.3 us
    pallas_call x1, Pallas kernels, shards(): pl.pallas_call(mix_kernel, out_shape=jax.ShapeDtypeStruct((rows, width +...  27.2 us
    ppermute x3, waiting for transfers between devices, to_partner(): return lax.ppermute(array, 'tp', [(i, (i + shift) % tp) for i in range(tp)])  14.5 us
    dot_general x7, matrix products, project(): jnp.dot(scaled, weight, preferred_element_type=jnp.float32) * inverse  8.45 us
    pallas_call x1, Pallas kernels, shards(): pl.pallas_call(local_kernel, out_shape=(jax.ShapeDtypeStruct((rows, narro...  4.19 us
    unnamed x24, local copies, waits for them, and re-layouts  3.23 us
    ppermute x3, starting transfers between devices, to_partner(): return lax.ppermute(array, 'tp', [(i, (i + shift) % tp) for i in range(tp)])  2.72 us
    dot_general x1, matrix products, shards(): jnp.dot(to_partner(heads, shift), out_weights[shift], preferred_element_t...  2.46 us
  transfers between devices with their start and end apart: 3, of which 2 were waited for; matrix products, arithmetic and copies ran while one was open for 4% of the time, Pallas kernels for 67%

profile of v2, /device:TPU:29, one launch (start us, length us, event | category | flops | bytes accessed | tf_op | source)
XLA Modules:
  0.0 104.7 jit_solution(6299197838975136882)
XLA Ops:
  0.0 0.0 copy-start
  0.0 1.2 %collective-permute-start = (bf16[256,1024]{1,0:T(8,128)(2,1)}, bf16[256,1024]{1,0:T(8,128)(2,1)S(1)}, u32[]{:S(2)}, u32[]{:S(2)}) collective-permute-start(bf16[256,1024]{1,0:T(8,128)(2,1)} %param.15), channel_id=1, source_target_pairs={{0,1},{1,0},{2,3},{3,2},{4,5},{5,4},{6,7},{7,6},{8,9},{9,8},{10,11... | collective-permute-start | bytes 1572872 | tf_op jit(solution)/shard_map/ppermute | solution.py:247
  1.2 1.5 %copy.16.spike_ref = f32[256,4]{1,0:T(8,128)} copy(f32[256,4]{0,1:T(4,128)} %param.26) | data formatting | bytes 8192 | tf_op args[11]
  2.7 0.0 copy-start.5
  2.7 0.0 copy-start.10
  2.7 0.1 broadcast_in_dim.2
  2.8 1.1 %constant_dynamic-update-slice_fusion.3 = bf16[256,2048]{1,0:T(8,128)(2,1)S(1)} fusion(bf16[256,2048]{1,0:T(8,128)(2,1)S(1)} %broadcast_in_dim.2, bf16[256,1024]{1,0:T(8,128)(2,1)} %param.15, s32[]{:T(128)S(6)} %select_n.10), kind=kLoop, calls=%fused_computation.28 | loop fusion | bytes 1048580 | tf_op jit(solution)/shard_map/dynamic_update_slice | solution.py:253
  4.0 9.1 %collective-permute-done = bf16[256,1024]{1,0:T(8,128)(2,1)S(1)} collective-permute-done((bf16[256,1024]{1,0:T(8,128)(2,1)}, bf16[256,1024]{1,0:T(8,128)(2,1)S(1)}, u32[]{:S(2)}, u32[]{:S(2)}) %collective-permute-start) | collective-permute-done | bytes 524320 | tf_op jit(solution)/shard_map/ppermute | solution.py:247
  13.1 0.3 fusion.1
  13.4 0.0 copy-done.5
  13.4 0.0 copy-done.10
  13.4 1.1 %fusion.8.v_ref = bf16[256,256]{1,0:T(8,128)(2,1)} fusion(bf16[2048,256]{1,0:T(8,128)(2,1)S(1)} %copy-done.5, bf16[256,2048]{1,0:T(8,128)(2,1)S(1)} %constant_dynamic-update-slice_fusion.2, f32[2048]{0:T(1024)S(1)} %copy-done.10, f32[256]{0:T(256)S(1)} %add_rsqrt_fusion), kind=kOutput, calls=%fused_computation.18 | convolution fusion | flops 270139392 | bytes 2237440 | tf_op jit(solution)/shard_map/dot_general | solution.py:271
  14.5 0.0 copy-done
  14.5 0.0 copy-start.4
  14.5 1.4 %fusion.4.f_ref = bf16[256,512]{1,0:T(8,128)(2,1)} fusion(bf16[2048,512]{1,0:T(8,128)(2,1)S(1)} %copy-done, bf16[256,2048]{1,0:T(8,128)(2,1)S(1)} %constant_dynamic-update-slice_fusion.2, f32[2048]{0:T(1024)S(1)} %copy-done.10, f32[256]{0:T(256)S(1)} %add_rsqrt_fusion), kind=kOutput, calls=%fused_computation.9 | convolution fusion | flops 538705920 | bytes 3417088 | tf_op jit(solution)/shard_map/dot_general | solution.py:271
  16.0 0.2 copy-done.4
  16.1 0.0 copy-start.6
  16.1 1.4 %fusion.3.q_ref = bf16[256,512]{1,0:T(8,128)(2,1)} fusion(bf16[2048,512]{1,0:T(8,128)(2,1)S(1)} %copy-done.4, bf16[256,2048]{1,0:T(8,128)(2,1)S(1)} %constant_dynamic-update-slice_fusion.2, f32[2048]{0:T(1024)S(1)} %copy-done.10, f32[256]{0:T(256)S(1)} %add_rsqrt_fusion), kind=kOutput, calls=%fused_computation.8 | convolution fusion | flops 538705920 | bytes 3417088 | tf_op jit(solution)/shard_map/dot_general | solution.py:271
  17.6 0.0 copy-done.6
  17.6 0.0 copy-start.7
  17.6 0.0 copy-start.8
  17.6 1.1 %fusion.7.value_ref = bf16[256,256]{1,0:T(8,128)(2,1)} fusion(bf16[2048,256]{1,0:T(8,128)(2,1)S(1)} %copy-done.6, bf16[256,2048]{1,0:T(8,128)(2,1)S(1)} %constant_dynamic-update-slice_fusion.2, f32[2048]{0:T(1024)S(1)} %copy-done.10, f32[256]{0:T(256)S(1)} %add_rsqrt_fusion), kind=kOutput, calls=%fused_computation.17 | convolution fusion | flops 270139392 | bytes 2237440 | tf_op jit(solution)/shard_map/dot_general | solution.py:271
  18.7 0.1 copy-done.7
  18.8 0.0 copy-start.9
  18.8 1.1 %fusion.6.key_ref = bf16[256,256]{1,0:T(8,128)(2,1)} fusion(bf16[2048,256]{1,0:T(8,128)(2,1)S(1)} %copy-done.7, bf16[256,2048]{1,0:T(8,128)(2,1)S(1)} %constant_dynamic-update-slice_fusion.2, f32[2048]{0:T(1024)S(1)} %copy-done.10, f32[256]{0:T(256)S(1)} %add_rsqrt_fusion), kind=kOutput, calls=%fused_computation.16 | convolution fusion | flops 270139392 | bytes 2237440 | tf_op jit(solution)/shard_map/dot_general | solution.py:271
  19.9 0.0 copy-done.8
  19.9 0.0 copy-start.2
  19.9 1.1 %fusion.9.gate_ref = bf16[256,256]{1,0:T(8,128)(2,1)} fusion(bf16[2048,256]{1,0:T(8,128)(2,1)S(1)} %copy-done.8, bf16[256,2048]{1,0:T(8,128)(2,1)S(1)} %constant_dynamic-update-slice_fusion.2, f32[2048]{0:T(1024)S(1)} %copy-done.10, f32[256]{0:T(256)S(1)} %add_rsqrt_fusion), kind=kOutput, calls=%fused_computation.19 | convolution fusion | flops 270139392 | bytes 2237440 | tf_op jit(solution)/shard_map/dot_general | solution.py:271
  21.0 0.0 copy-done.9
  21.0 0.0 copy-start.3
  21.0 1.1 %fusion.5.q_ref = bf16[256,256]{1,0:T(8,128)(2,1)} fusion(bf16[2048,256]{1,0:T(8,128)(2,1)S(1)} %copy-done.9, bf16[256,2048]{1,0:T(8,128)(2,1)S(1)} %constant_dynamic-update-slice_fusion.2, f32[2048]{0:T(1024)S(1)} %copy-done.10, f32[256]{0:T(256)S(1)} %add_rsqrt_fusion), kind=kOutput, calls=%fused_computation.15 | convolution fusion | flops 270139392 | bytes 2237440 | tf_op jit(solution)/shard_map/dot_general | solution.py:271
  22.1 0.0 copy-done.2
  22.1 0.1 constant_dynamic-update-slice_fusion.1
  22.2 0.0 copy-done.3
  22.3 0.1 constant_dynamic-update-slice_fusion
  22.4 0.0 copy-start.1
  22.4 1.3 %copy-done.1 = bf16[512,2048]{1,0:T(8,128)(2,1)} copy-done((bf16[512,2048]{1,0:T(8,128)(2,1)}, bf16[512,2048]{1,0:T(8,128)(2,1)S(1)}, u32[]{:S(2)}) %copy-start.1) | copy-done | bytes 2097176
  23.7 0.1 constant_dynamic-slice_fusion
  23.8 1.3 %collective-permute-start.2 = (bf16[512,1024]{1,0:T(8,128)(2,1)S(1)}, bf16[512,1024]{1,0:T(8,128)(2,1)}, u32[]{:S(2)}, u32[]{:S(2)}) collective-permute-start(bf16[512,1024]{1,0:T(8,128)(2,1)S(1)} %constant_dynamic-slice_fusion), channel_id=1, source_target_pairs={{0,1},{1,0},{2,3},{3,2},{4,5},{5,4},{6,7},{7,6},{8,9},{9,8},{10,11... | collective-permute-start | bytes 3145736 | tf_op jit(solution)/shard_map/ppermute | solution.py:247
  25.1 4.2 %recurrence_local.1 = (f32[256,256]{1,0:T(8,128)}, bf16[256,512]{1,0:T(8,128)(2,1)}, bf16[336,512]{1,0:T(8,128)(2,1)}) custom-call(bf16[256,256]{1,0:T(8,128)(2,1)} %fusion.6.key_ref, bf16[256,256]{1,0:T(8,128)(2,1)} %fusion.7.value_ref, bf16[256,512]{1,0:T(8,128)(2,1)} %fusion.3.q_ref, bf16[256,512]{1,0:T(8,128)(2,1)} %fusion.4.f_ref, ...), custom_call_target="tpu_custom_call" | custom-call | flops 1000000000 | bytes 2000000 | tf_op jit(solution)/shard_map/recurrence_local/pallas_call | solution.py:278
  29.3 38.3 %gather_earlier.1.kv_ref = bf16[16,336,512]{2,1,0:T(8,128)(2,1)} custom-call(bf16[336,512]{1,0:T(8,128)(2,1)} %get-tuple-element.12.in_ref), custom_call_target="tpu_custom_call" | custom-call | flops 10000000000 | bytes 100000000 | tf_op jit(solution)/shard_map/gather_earlier/pallas_call | solution.py:299
  67.6 27.2 %mix_heads.1 = bf16[256,512]{1,0:T(8,128)(2,1)} custom-call(f32[4]{0:T(128)} %bias_ref.1, bf16[256,256]{1,0:T(8,128)(2,1)} %fusion.5.q_ref, bf16[16,336,512]{2,1,0:T(8,128)(2,1)} %gather_earlier.1.kv_ref, f32[256,256]{1,0:T(8,128)} %get-tuple-element.13.local_ref, bf16[256,512]{1,0:T(8,128)(2,1)} %get-tuple-element.14.qdec_ref, ...), custom_call_target="tpu_custom_call" | custom-call | tf_op jit(solution)/shard_map/mix_heads/pallas_call | solution.py:315
  94.8 0.2 collective-permute-start.1
  95.1 1.7 %fusion.10 = f32[256,1024]{1,0:T(8,128)S(1)} fusion(bf16[256,512]{1,0:T(8,128)(2,1)} %mix_heads.1, bf16[512,2048]{1,0:T(8,128)(2,1)} %copy-done.1, s32[]{:T(128)S(6)} %select_n.12), kind=kOutput, calls=%fused_computation.20 | convolution fusion | flops 268435456 | bytes 2359300 | tf_op jit(solution)/shard_map/dot_general | solution.py:336
  96.8 5.4 %collective-permute-done.1 = bf16[256,512]{1,0:T(8,128)(2,1)S(1)} collective-permute-done((bf16[256,512]{1,0:T(8,128)(2,1)}, bf16[256,512]{1,0:T(8,128)(2,1)S(1)}, u32[]{:S(2)}, u32[]{:S(2)}) %collective-permute-start.1) | collective-permute-done | bytes 262176 | tf_op jit(solution)/shard_map/ppermute | solution.py:247
  102.2 0.0 collective-permute-done.2
  102.2 2.5 %fusion.2 = bf16[256,1024]{1,0:T(8,128)(2,1)} fusion(f32[256,1024]{1,0:T(8,128)S(1)} %fusion.10, bf16[256,512]{1,0:T(8,128)(2,1)S(1)} %collective-permute-done.1, bf16[512,1024]{1,0:T(8,128)(2,1)} %collective-permute-done.2), kind=kOutput, calls=%fused_computation.5 | convolution fusion | flops 268959744 | bytes 2883584 | tf_op jit(solution)/shard_map/dot_general | solution.py:338
  (2 shorter events, 0.1 us)
Async XLA Ops:
  0.0 14.5 %copy-start = (bf16[2048,512]{1,0:T(8,128)(2,1)S(1)}, bf16[2048,512]{1,0:T(8,128)(2,1)}, u32[]{:S(2)}) copy-start(bf16[2048,512]{1,0:T(8,128)(2,1)} %param.22) | copy-start | bytes 6291460
  0.0 13.0 %collective-permute-start = (bf16[256,1024]{1,0:T(8,128)(2,1)}, bf16[256,1024]{1,0:T(8,128)(2,1)S(1)}, u32[]{:S(2)}, u32[]{:S(2)}) collective-permute-start(bf16[256,1024]{1,0:T(8,128)(2,1)} %param.15), channel_id=1, source_target_pairs={{0,1},{1,0},{2,3},{3,2},{4,5},{5,4},{6,7},{7,6},{8,9},{9,8},{10,11... | collective-permute-start | bytes 1572872 | tf_op jit(solution)/shard_map/ppermute | solution.py:247
  2.7 10.7 %copy-start.5 = (bf16[2048,256]{1,0:T(8,128)(2,1)S(1)}, bf16[2048,256]{1,0:T(8,128)(2,1)}, u32[]{:S(2)}) copy-start(bf16[2048,256]{1,0:T(8,128)(2,1)} %param.23) | copy-start | bytes 3145732
  2.7 10.7 %copy-start.10 = (f32[2048]{0:T(1024)S(1)}, f32[2048]{0:T(1024)}, u32[]{:S(2)}) copy-start(f32[2048]{0:T(1024)} %param.16) | copy-start | bytes 24580
  14.5 1.6 %copy-start.4 = (bf16[2048,512]{1,0:T(8,128)(2,1)S(1)}, bf16[2048,512]{1,0:T(8,128)(2,1)}, u32[]{:S(2)}) copy-start(bf16[2048,512]{1,0:T(8,128)(2,1)} %param.21) | copy-start | bytes 6291460
  16.1 1.5 %copy-start.6 = (bf16[2048,256]{1,0:T(8,128)(2,1)S(1)}, bf16[2048,256]{1,0:T(8,128)(2,1)}, u32[]{:S(2)}) copy-start(bf16[2048,256]{1,0:T(8,128)(2,1)} %param.19) | copy-start | bytes 3145732
  17.6 1.2 %copy-start.7 = (bf16[2048,256]{1,0:T(8,128)(2,1)S(1)}, bf16[2048,256]{1,0:T(8,128)(2,1)}, u32[]{:S(2)}) copy-start(bf16[2048,256]{1,0:T(8,128)(2,1)} %param.18) | copy-start | bytes 3145732
  17.6 2.3 %copy-start.8 = (bf16[2048,256]{1,0:T(8,128)(2,1)S(1)}, bf16[2048,256]{1,0:T(8,128)(2,1)}, u32[]{:S(2)}) copy-start(bf16[2048,256]{1,0:T(8,128)(2,1)} %param.24) | copy-start | bytes 3145732
  18.8 2.2 %copy-start.9 = (bf16[2048,256]{1,0:T(8,128)(2,1)S(1)}, bf16[2048,256]{1,0:T(8,128)(2,1)}, u32[]{:S(2)}) copy-start(bf16[2048,256]{1,0:T(8,128)(2,1)} %param.17) | copy-start | bytes 3145732
  19.9 2.2 %copy-start.2 = (bf16[256,2048]{1,0:T(8,128)(2,1)S(1)}, bf16[256,2048]{1,0:T(8,128)(2,1)}, u32[]{:S(2)}) copy-start(bf16[256,2048]{1,0:T(8,128)(2,1)} %param.28) | copy-start | bytes 3145732
  21.0 1.3 %copy-start.3 = (bf16[256,2048]{1,0:T(8,128)(2,1)S(1)}, bf16[256,2048]{1,0:T(8,128)(2,1)}, u32[]{:S(2)}) copy-start(bf16[256,2048]{1,0:T(8,128)(2,1)} %param.29) | copy-start | bytes 3145732
  22.4 1.3 %copy-start.1 = (bf16[512,2048]{1,0:T(8,128)(2,1)}, bf16[512,2048]{1,0:T(8,128)(2,1)S(1)}, u32[]{:S(2)}) copy-start(bf16[512,2048]{1,0:T(8,128)(2,1)S(1)} %constant_dynamic-update-slice_fusion) | copy-start | bytes 6291460
  23.8 78.4 %collective-permute-start.2 = (bf16[512,1024]{1,0:T(8,128)(2,1)S(1)}, bf16[512,1024]{1,0:T(8,128)(2,1)}, u32[]{:S(2)}, u32[]{:S(2)}) collective-permute-start(bf16[512,1024]{1,0:T(8,128)(2,1)S(1)} %constant_dynamic-slice_fusion), channel_id=1, source_target_pairs={{0,1},{1,0},{2,3},{3,2},{4,5},{5,4},{6,7},{7,6},{8,9},{9,8},{10,11... | collective-permute-start | bytes 3145736 | tf_op jit(solution)/shard_map/ppermute | solution.py:247
  94.8 7.4 %collective-permute-start.1 = (bf16[256,512]{1,0:T(8,128)(2,1)}, bf16[256,512]{1,0:T(8,128)(2,1)S(1)}, u32[]{:S(2)}, u32[]{:S(2)}) collective-permute-start(bf16[256,512]{1,0:T(8,128)(2,1)} %mix_heads.1), channel_id=1, source_target_pairs={{0,1},{1,0},{2,3},{3,2},{4,5},{5,4},{6,7},{7,6},{8,9},{9,8},{10,11... | collective-permute-start | bytes 786440 | tf_op jit(solution)/shard_map/ppermute | solution.py:247

commit v3 on v2

--- a/solution.py
+++ b/solution.py
@@ -247,12 +247,9 @@
         return lax.ppermute(array, "tp", [(i, (i + shift) % tp) for i in range(tp)])
 
     features = tokens.shape[1]
-    values = jnp.zeros((rows, features * tp), tokens.dtype)
-    for shift in range(tp):
-        piece = tokens if shift == 0 else to_partner(tokens, shift)
-        values = lax.dynamic_update_slice_in_dim(values, piece, lax.rem(mine + tp - shift, tp) * features, 1)
-    attention_output_weight, recurrence_output_weight, values = lax.optimization_barrier(
-        (attention_output_weight, recurrence_output_weight, values)
+    pieces = [tokens] + [to_partner(tokens, shift) for shift in range(1, tp)]
+    attention_output_weight, recurrence_output_weight, pieces[-1] = lax.optimization_barrier(
+        (attention_output_weight, recurrence_output_weight, pieces[-1])
     )
     own_rows = jnp.concatenate([attention_output_weight, recurrence_output_weight], axis=0)
     columns = own_rows.shape[1] // tp
@@ -262,13 +259,21 @@
 
     out_weights = [cut(0)] + [to_partner(cut(shift), shift) for shift in range(1, tp)]
 
-    values = values.astype(jnp.float32)
-    scaled = (values * input_norm_gain[None, :]).astype(jnp.bfloat16)
-    squares = jnp.mean(values * values, axis=1)
+    starts = [lax.rem(mine + tp - shift, tp) * features for shift in range(tp)]
+    values = [piece.astype(jnp.float32) for piece in pieces]
+    scaled = [
+        (value * lax.dynamic_slice_in_dim(input_norm_gain, start, features, 0)[None, :]).astype(jnp.bfloat16)
+        for value, start in zip(values, starts)
+    ]
+    squares = sum(jnp.sum(value * value, axis=1) for value in values) / (features * tp)
     inverse = lax.rsqrt(squares + epsilon)[:, None]
 
     def project(weight):
-        return (jnp.dot(scaled, weight, preferred_element_type=jnp.float32) * inverse).astype(jnp.bfloat16)
+        total = sum(
+            jnp.dot(part, lax.dynamic_slice_in_dim(weight, start, features, 0), preferred_element_type=jnp.float32)
+            for part, start in zip(scaled, starts)
+        )
+        return (total * inverse).astype(jnp.bfloat16)
 
     key_stick, value_stick = project(attention_key_weight), project(attention_value_weight)
     query_rows, forget_rows = project(recurrence_query_weight), project(forget_weight)

time: 105 us -> 103 us (0.981)
  waiting for transfers between devices: 14.5 us -> 6.41 us
  matrix products: 12.6 us -> 19.2 us
    ppermute x3, waiting for transfers between devices: 14.5 us -> 6.41 us  [to_partner(): return lax.ppermute(array, 'tp', [(i, (i + shift) % tp) for i in range(tp)])]
    dot_general x7 -> x14, matrix products: 8.45 us -> 15 us  [project(): jnp.dot(part, lax.dynamic_slice_in_dim(weight, start, features, 0), prefe...]
    dynamic_update_slice x2 -> x0, local copies, waits for them, and re-layouts: 1.2 us -> none  [shards(): lax.dynamic_update_slice_in_dim(values, piece, lax.rem(mine + tp - shift,...]
    unnamed x24 -> x40, local copies, waits for them, and re-layouts: 3.23 us -> 3.55 us
  transfers between devices with their start and end apart: 3 -> 3, of which waited for: 2 -> 2; matrix products, arithmetic and copies ran while one was open for 4% -> 11% of each run, Pallas kernels for 67% -> 68%
where the time goes in v3:
time: 103 us
  Pallas kernels  69.7 us (68%)
  matrix products  19.2 us (19%)
  waiting for transfers between devices  6.41 us (6%)
  local copies, waits for them, and re-layouts  4.59 us (4%)
  starting transfers between devices  2.73 us (3%)
    pallas_call x1, Pallas kernels, shards(): pl.pallas_call(functools.partial(gather_kernel, sp // 4), out_shape=jax.S...  38.3 us
    pallas_call x1, Pallas kernels, shards(): pl.pallas_call(mix_kernel, out_shape=jax.ShapeDtypeStruct((rows, width +...  27.2 us
    dot_general x14, matrix products, project(): jnp.dot(part, lax.dynamic_slice_in_dim(weight, start, features, 0), prefe...  15 us
    ppermute x3, waiting for transfers between devices, to_partner(): return lax.ppermute(array, 'tp', [(i, (i + shift) % tp) for i in range(tp)])  6.41 us
    pallas_call x1, Pallas kernels, shards(): pl.pallas_call(local_kernel, out_shape=(jax.ShapeDtypeStruct((rows, narro...  4.18 us
    unnamed x40, local copies, waits for them, and re-layouts  3.55 us
    ppermute x3, starting transfers between devices, to_partner(): return lax.ppermute(array, 'tp', [(i, (i + shift) % tp) for i in range(tp)])  2.73 us
    dot_general x1, matrix products, shards(): jnp.dot(to_partner(heads, shift), out_weights[shift], preferred_element_t...  2.46 us
  transfers between devices with their start and end apart: 3, of which 2 were waited for; matrix products, arithmetic and copies ran while one was open for 11% of the time, Pallas kernels for 68%

profile of v3, /device:TPU:29, one launch (start us, length us, event | category | flops | bytes accessed | tf_op | source)
XLA Modules:
  0.0 103.1 jit_solution(15564405540854462081)
XLA Ops:
  0.0 0.0 copy-start
  0.0 0.0 copy-start.1
  0.0 1.2 %collective-permute-start = (bf16[256,1024]{1,0:T(8,128)(2,1)}, bf16[256,1024]{1,0:T(8,128)(2,1)S(1)}, u32[]{:S(2)}, u32[]{:S(2)}) collective-permute-start(bf16[256,1024]{1,0:T(8,128)(2,1)} %param.15), channel_id=1, source_target_pairs={{0,1},{1,0},{2,3},{3,2},{4,5},{5,4},{6,7},{7,6},{8,9},{9,8},{10,11... | collective-permute-start | bytes 1572872 | tf_op jit(solution)/shard_map/ppermute | solution.py:247
  1.2 0.0 copy-start.8
  1.2 0.0 copy-start.10
  1.2 0.9 fusion.71
  2.1 2.2 %fusion.31 = f32[256,256]{1,0:T(8,128)} fusion(bf16[2048,256]{1,0:T(8,128)(2,1)} %param.23, s32[]{:T(128)S(6)} %select_n.6, bf16[256,1024]{1,0:T(8,128)(2,1)} %param.15, f32[1024]{0:T(1024)S(1)} %get-tuple-element.18), kind=kOutput, calls=%fused_computation.43 | convolution fusion | flops 135004160 | bytes 1314820 | tf_op jit(solution)/shard_map/dot_general | solution.py:273
  4.3 2.3 %fusion.34 = f32[256,256]{1,0:T(8,128)} fusion(bf16[2048,256]{1,0:T(8,128)(2,1)} %param.19, s32[]{:T(128)S(6)} %select_n.6, bf16[256,1024]{1,0:T(8,128)(2,1)} %param.15, f32[1024]{0:T(1024)S(1)} %get-tuple-element.18), kind=kOutput, calls=%fused_computation.46 | convolution fusion | flops 135004160 | bytes 1314820 | tf_op jit(solution)/shard_map/dot_general | solution.py:273
  6.6 0.0 copy-done.1
  6.6 0.0 copy-done.8
  6.6 0.0 copy-start.18
  6.6 1.0 fusion.37
  7.6 0.0 copy-done.10
  7.6 1.0 fusion.28
  8.7 0.0 copy-done.12
  8.7 0.3 fusion.40
  9.0 0.2 fusion.16
  9.2 0.0 copy-done.18
  9.2 0.8 copy.16.spike_ref
  10.0 0.0 copy-done
  10.0 0.0 copy-start.3
  10.0 0.4 fusion.22
  10.4 1.1 %copy-done.3 = bf16[2048,512]{1,0:T(8,128)(2,1)S(1)} copy-done((bf16[2048,512]{1,0:T(8,128)(2,1)S(1)}, bf16[2048,512]{1,0:T(8,128)(2,1)}, u32[]{:S(2)}) %copy-start.3) | copy-done | bytes 2097176
  11.6 0.4 fusion.25
  12.0 1.0 collective-permute-done
  13.0 0.2 fusion.18
  13.2 0.0 copy-start.6
  13.2 0.0 copy-start.17
  13.2 1.2 %fusion.3.f_ref = bf16[256,512]{1,0:T(8,128)(2,1)} fusion(f32[256,512]{1,0:T(8,128)S(1)} %fusion.22, bf16[2048,512]{1,0:T(8,128)(2,1)S(1)} %copy-done, s32[]{:T(128)S(6)} %select_n.7, f32[256]{0:T(256)S(1)} %add_rsqrt_fusion, bf16[256,1024]{1,0:T(8,128)(2,1)S(1)} %collective-permute-done, f32[1024]{0:T(1024)S(1)} %get-tuple-element.17), kind=kOutput, calls=%fused_computation.10 | convolution fusion | flops 269615104 | bytes 2364420 | tf_op jit(solution)/shard_map/dot_general | solution.py:273
  14.4 0.0 copy-start.7
  14.4 0.0 copy-start.16
  14.4 0.0 copy-start.9
  14.4 0.0 copy-start.15
  14.4 1.2 %fusion.4.q_ref = bf16[256,512]{1,0:T(8,128)(2,1)} fusion(f32[256,512]{1,0:T(8,128)S(1)} %fusion.25, bf16[2048,512]{1,0:T(8,128)(2,1)S(1)} %copy-done.3, s32[]{:T(128)S(6)} %select_n.7, f32[256]{0:T(256)S(1)} %add_rsqrt_fusion, bf16[256,1024]{1,0:T(8,128)(2,1)S(1)} %collective-permute-done, f32[1024]{0:T(1024)S(1)} %get-tuple-element.17), kind=kOutput, calls=%fused_computation.11 | convolution fusion | flops 269615104 | bytes 2364420 | tf_op jit(solution)/shard_map/dot_general | solution.py:273
  15.6 0.0 copy-done.6
  15.6 0.0 copy-done.17
  15.6 1.0 fusion.11.v_ref
  16.6 0.0 copy-done.7
  16.6 0.0 copy-done.16
  16.6 1.0 fusion.12.value_ref
  17.6 0.0 copy-done.9
  17.6 0.0 copy-done.15
  17.6 1.0 fusion.13.key_ref
  18.5 0.0 copy-done.11
  18.5 0.0 copy-done.14
  18.5 1.0 fusion.10.gate_ref
  19.5 0.0 copy-done.13
  19.5 1.0 fusion.14.q_ref
  20.5 0.0 copy-done.4
  20.5 0.1 constant_dynamic-update-slice_fusion.1
  20.6 0.1 copy-done.5
  20.7 0.1 constant_dynamic-update-slice_fusion
  20.9 0.0 copy-start.2
  20.9 1.3 %copy-done.2 = bf16[512,2048]{1,0:T(8,128)(2,1)} copy-done((bf16[512,2048]{1,0:T(8,128)(2,1)}, bf16[512,2048]{1,0:T(8,128)(2,1)S(1)}, u32[]{:S(2)}) %copy-start.2) | copy-done | bytes 2097176
  22.2 0.1 constant_dynamic-slice_fusion
  22.3 1.3 %collective-permute-start.2 = (bf16[512,1024]{1,0:T(8,128)(2,1)S(1)}, bf16[512,1024]{1,0:T(8,128)(2,1)}, u32[]{:S(2)}, u32[]{:S(2)}) collective-permute-start(bf16[512,1024]{1,0:T(8,128)(2,1)S(1)} %constant_dynamic-slice_fusion), channel_id=1, source_target_pairs={{0,1},{1,0},{2,3},{3,2},{4,5},{5,4},{6,7},{7,6},{8,9},{9,8},{10,11... | collective-permute-start | bytes 3145736 | tf_op jit(solution)/shard_map/ppermute | solution.py:247
  23.6 4.2 %recurrence_local.1 = (f32[256,256]{1,0:T(8,128)}, bf16[256,512]{1,0:T(8,128)(2,1)}, bf16[336,512]{1,0:T(8,128)(2,1)}) custom-call(bf16[256,256]{1,0:T(8,128)(2,1)} %fusion.13.key_ref, bf16[256,256]{1,0:T(8,128)(2,1)} %fusion.12.value_ref, bf16[256,512]{1,0:T(8,128)(2,1)} %fusion.4.q_ref, bf16[256,512]{1,0:T(8,128)(2,1)} %fusion.3.f_ref, ...), custom_call_target="tpu_custom_call" | custom-call | flops 1000000000 | bytes 2000000 | tf_op jit(solution)/shard_map/recurrence_local/pallas_call | solution.py:283
  27.7 38.3 %gather_earlier.1.kv_ref = bf16[16,336,512]{2,1,0:T(8,128)(2,1)} custom-call(bf16[336,512]{1,0:T(8,128)(2,1)} %get-tuple-element.12.in_ref), custom_call_target="tpu_custom_call" | custom-call | flops 10000000000 | bytes 100000000 | tf_op jit(solution)/shard_map/gather_earlier/pallas_call | solution.py:304
  66.1 27.2 %mix_heads.1 = bf16[256,512]{1,0:T(8,128)(2,1)} custom-call(f32[4]{0:T(128)} %bias_ref.1, bf16[256,256]{1,0:T(8,128)(2,1)} %fusion.14.q_ref, bf16[16,336,512]{2,1,0:T(8,128)(2,1)} %gather_earlier.1.kv_ref, f32[256,256]{1,0:T(8,128)} %get-tuple-element.13.local_ref, bf16[256,512]{1,0:T(8,128)(2,1)} %get-tuple-element.14.qdec_ref, ...), custom_call_target="tpu_custom_call" | custom-call | tf_op jit(solution)/shard_map/mix_heads/pallas_call | solution.py:320
  93.2 0.2 collective-permute-start.1
  93.5 1.7 %fusion.19 = f32[256,1024]{1,0:T(8,128)S(1)} fusion(bf16[256,512]{1,0:T(8,128)(2,1)} %mix_heads.1, bf16[512,2048]{1,0:T(8,128)(2,1)} %copy-done.2, s32[]{:T(128)S(6)} %select_n.8), kind=kOutput, calls=%fused_computation.31 | convolution fusion | flops 268435456 | bytes 2359300 | tf_op jit(solution)/shard_map/dot_general | solution.py:341
  95.2 5.4 %collective-permute-done.1 = bf16[256,512]{1,0:T(8,128)(2,1)S(1)} collective-permute-done((bf16[256,512]{1,0:T(8,128)(2,1)}, bf16[256,512]{1,0:T(8,128)(2,1)S(1)}, u32[]{:S(2)}, u32[]{:S(2)}) %collective-permute-start.1) | collective-permute-done | bytes 262176 | tf_op jit(solution)/shard_map/ppermute | solution.py:247
  100.6 0.0 collective-permute-done.2
  100.6 2.5 %fusion = bf16[256,1024]{1,0:T(8,128)(2,1)} fusion(f32[256,1024]{1,0:T(8,128)S(1)} %fusion.19, bf16[256,512]{1,0:T(8,128)(2,1)S(1)} %collective-permute-done.1, bf16[512,1024]{1,0:T(8,128)(2,1)} %collective-permute-done.2), kind=kOutput, calls=%fused_computation.5 | convolution fusion | flops 268959744 | bytes 2883584 | tf_op jit(solution)/shard_map/dot_general | solution.py:343
  (7 shorter events, 0.0 us)
Async XLA Ops:
  0.0 10.0 %copy-start = (bf16[2048,512]{1,0:T(8,128)(2,1)S(1)}, bf16[2048,512]{1,0:T(8,128)(2,1)}, u32[]{:S(2)}) copy-start(bf16[2048,512]{1,0:T(8,128)(2,1)} %param.22) | copy-start | bytes 6291460
  0.0 6.6 %copy-start.1 = (bf16[256,1024]{1,0:T(8,128)(2,1)S(1)}, bf16[256,1024]{1,0:T(8,128)(2,1)}, u32[]{:S(2)}) copy-start(bf16[256,1024]{1,0:T(8,128)(2,1)} %param.15) | copy-start | bytes 1572868
  0.0 13.0 %collective-permute-start = (bf16[256,1024]{1,0:T(8,128)(2,1)}, bf16[256,1024]{1,0:T(8,128)(2,1)S(1)}, u32[]{:S(2)}, u32[]{:S(2)}) collective-permute-start(bf16[256,1024]{1,0:T(8,128)(2,1)} %param.15), channel_id=1, source_target_pairs={{0,1},{1,0},{2,3},{3,2},{4,5},{5,4},{6,7},{7,6},{8,9},{9,8},{10,11... | collective-permute-start | bytes 1572872 | tf_op jit(solution)/shard_map/ppermute | solution.py:247
  1.2 5.4 %copy-start.8 = (bf16[2048,256]{1,0:T(8,128)(2,1)S(1)}, bf16[2048,256]{1,0:T(8,128)(2,1)}, u32[]{:S(2)}) copy-start(bf16[2048,256]{1,0:T(8,128)(2,1)} %param.18) | copy-start | bytes 3145732
  1.2 6.4 %copy-start.10 = (bf16[2048,256]{1,0:T(8,128)(2,1)S(1)}, bf16[2048,256]{1,0:T(8,128)(2,1)}, u32[]{:S(2)}) copy-start(bf16[2048,256]{1,0:T(8,128)(2,1)} %param.24) | copy-start | bytes 3145732
  4.3 4.4 %copy-start.12 = (bf16[2048,256]{1,0:T(8,128)(2,1)S(1)}, bf16[2048,256]{1,0:T(8,128)(2,1)}, u32[]{:S(2)}) copy-start(bf16[2048,256]{1,0:T(8,128)(2,1)} %param.17) | copy-start | bytes 3145732
  6.6 2.6 %copy-start.18 = (f32[256,4]{0,1:T(4,128)S(1)}, f32[256,4]{0,1:T(4,128)}, u32[]{:S(2)}) copy-start(f32[256,4]{0,1:T(4,128)} %param.26) | copy-start | bytes 12292
  10.0 1.6 %copy-start.3 = (bf16[2048,512]{1,0:T(8,128)(2,1)S(1)}, bf16[2048,512]{1,0:T(8,128)(2,1)}, u32[]{:S(2)}) copy-start(bf16[2048,512]{1,0:T(8,128)(2,1)} %param.21) | copy-start | bytes 6291460
  13.2 2.4 %copy-start.6 = (bf16[2048,256]{1,0:T(8,128)(2,1)S(1)}, bf16[2048,256]{1,0:T(8,128)(2,1)}, u32[]{:S(2)}) copy-start(bf16[2048,256]{1,0:T(8,128)(2,1)} %param.23) | copy-start | bytes 3145732
  13.2 2.4 %copy-start.17 = (f32[256,256]{1,0:T(8,128)S(1)}, f32[256,256]{1,0:T(8,128)}, u32[]{:S(2)}) copy-start(f32[256,256]{1,0:T(8,128)} %fusion.31) | copy-start | bytes 786436
  14.4 2.2 %copy-start.7 = (bf16[2048,256]{1,0:T(8,128)(2,1)S(1)}, bf16[2048,256]{1,0:T(8,128)(2,1)}, u32[]{:S(2)}) copy-start(bf16[2048,256]{1,0:T(8,128)(2,1)} %param.19) | copy-start | bytes 3145732
  14.4 2.2 %copy-start.16 = (f32[256,256]{1,0:T(8,128)S(1)}, f32[256,256]{1,0:T(8,128)}, u32[]{:S(2)}) copy-start(f32[256,256]{1,0:T(8,128)} %fusion.34) | copy-start | bytes 786436
  14.4 3.2 %copy-start.9 = (bf16[2048,256]{1,0:T(8,128)(2,1)S(1)}, bf16[2048,256]{1,0:T(8,128)(2,1)}, u32[]{:S(2)}) copy-start(bf16[2048,256]{1,0:T(8,128)(2,1)} %param.18) | copy-start | bytes 3145732
  14.4 3.2 %copy-start.15 = (f32[256,256]{1,0:T(8,128)S(1)}, f32[256,256]{1,0:T(8,128)}, u32[]{:S(2)}) copy-start(f32[256,256]{1,0:T(8,128)} %fusion.37) | copy-start | bytes 786436
  15.6 2.9 %copy-start.11 = (bf16[2048,256]{1,0:T(8,128)(2,1)S(1)}, bf16[2048,256]{1,0:T(8,128)(2,1)}, u32[]{:S(2)}) copy-start(bf16[2048,256]{1,0:T(8,128)(2,1)} %param.24) | copy-start | bytes 3145732
  15.6 2.9 %copy-start.14 = (f32[256,256]{1,0:T(8,128)S(1)}, f32[256,256]{1,0:T(8,128)}, u32[]{:S(2)}) copy-start(f32[256,256]{1,0:T(8,128)} %fusion.28) | copy-start | bytes 786436
  16.6 2.9 %copy-start.13 = (bf16[2048,256]{1,0:T(8,128)(2,1)S(1)}, bf16[2048,256]{1,0:T(8,128)(2,1)}, u32[]{:S(2)}) copy-start(bf16[2048,256]{1,0:T(8,128)(2,1)} %param.17) | copy-start | bytes 3145732
  17.6 2.9 %copy-start.4 = (bf16[256,2048]{1,0:T(8,128)(2,1)S(1)}, bf16[256,2048]{1,0:T(8,128)(2,1)}, u32[]{:S(2)}) copy-start(bf16[256,2048]{1,0:T(8,128)(2,1)} %param.28) | copy-start | bytes 3145732
  19.5 1.2 %copy-start.5 = (bf16[256,2048]{1,0:T(8,128)(2,1)S(1)}, bf16[256,2048]{1,0:T(8,128)(2,1)}, u32[]{:S(2)}) copy-start(bf16[256,2048]{1,0:T(8,128)(2,1)} %param.29) | copy-start | bytes 3145732
  20.9 1.3 %copy-start.2 = (bf16[512,2048]{1,0:T(8,128)(2,1)}, bf16[512,2048]{1,0:T(8,128)(2,1)S(1)}, u32[]{:S(2)}) copy-start(bf16[512,2048]{1,0:T(8,128)(2,1)S(1)} %constant_dynamic-update-slice_fusion) | copy-start | bytes 6291460
  22.3 78.4 %collective-permute-start.2 = (bf16[512,1024]{1,0:T(8,128)(2,1)S(1)}, bf16[512,1024]{1,0:T(8,128)(2,1)}, u32[]{:S(2)}, u32[]{:S(2)}) collective-permute-start(bf16[512,1024]{1,0:T(8,128)(2,1)S(1)} %constant_dynamic-slice_fusion), channel_id=1, source_target_pairs={{0,1},{1,0},{2,3},{3,2},{4,5},{5,4},{6,7},{7,6},{8,9},{9,8},{10,11... | collective-permute-start | bytes 3145736 | tf_op jit(solution)/shard_map/ppermute | solution.py:247
  93.2 7.4 %collective-permute-start.1 = (bf16[256,512]{1,0:T(8,128)(2,1)}, bf16[256,512]{1,0:T(8,128)(2,1)S(1)}, u32[]{:S(2)}, u32[]{:S(2)}) collective-permute-start(bf16[256,512]{1,0:T(8,128)(2,1)} %mix_heads.1), channel_id=1, source_target_pairs={{0,1},{1,0},{2,3},{3,2},{4,5},{5,4},{6,7},{7,6},{8,9},{9,8},{10,11... | collective-permute-start | bytes 786440 | tf_op jit(solution)/shard_map/ppermute | solution.py:247
